TPU v7x, 256 devices: a whole 4x4x8 slice. The times are simulated.
256 devices in a mesh: sp: 32 (over z, x), tp: 8 (over y, core).
Axes of the slice: x: 4, y: 4, z: 8, core: 2. Of those that a mesh axis runs over, the one named last changes fastest.
Arguments:
- block_input: bfloat16 [8192, 2048], P('sp'), may hold values from -12 to 12
- queries: bfloat16 [8192, 1024], P('sp', 'tp'), may hold values from -6 to 6
- keys: bfloat16 [8192, 1024], P('sp', 'tp'), may hold values from -6 to 6
- w_value: bfloat16 [2048, 2048], P(None, 'tp'), may hold values from -0.125 to 0.125
- log_decay: float32 [8192, 1024], P('sp', 'tp'), as said below
- d_out: bfloat16 [8192, 2048], P('sp', 'tp'), may hold values from -0.0625 to 0.0625
Outputs:
- d_queries: bfloat16 [8192, 1024], P('sp', 'tp')
- d_keys: bfloat16 [8192, 1024], P('sp', 'tp')
- d_log_decay: float32 [8192, 1024], P('sp', 'tp')
- d_w_value: float32 [2048, 2048], P('sp', 'tp')
- row_norms: float32 [2048], P('sp')
Inputs may be any that keep to these rules, and one draw needn't show every extreme that they name: log_decay is negative; key channels differ in rate, and rates change along the sequence.
All inputs are finite; a program needn't handle non-finite values.
Results may differ from a plain program's by a relative error of at most 0.015.
Values sent between devices are 32-bit elements; how exact they have to be, the bound alone decides.
A program may use at most 64 MiB of HBM per device.

v0:
```python
import jax
import jax.numpy as jnp
from jax import lax
from jax.sharding import Mesh
from jax.sharding import PartitionSpec as P

DK = 128
DV = 256
SP = ("sp_0", "sp_1")


def nothing_yet(value, identity):
    return jax.tree.map(
        lambda part, zero: jnp.zeros_like(part) + jnp.asarray(zero, part.dtype), value, identity
    )


def prefix_by_axis(value, axes, combine, identity, reverse):
    before = start = nothing_yet(value, identity)
    subtotal = value
    for axis in reversed(axes):
        size, place = (lax.axis_size(axis), lax.axis_index(axis))
        pieces = jax.tree.map(lambda part: lax.all_gather(part, axis), subtotal)
        inside, subtotal = (start, start)
        for k in reversed(range(size)) if reverse else range(size):
            passed = k > place if reverse else k < place
            subtotal = combine(subtotal, jax.tree.map(lambda part: part[k], pieces))
            inside = jax.tree.map(lambda new, old: jnp.where(passed, new, old), subtotal, inside)
        before = combine(inside, before)
    return before


def split_up(value, dim, size):
    before, after = (value.shape[:dim], value.shape[dim + 1 :])
    return jnp.moveaxis(value.reshape(*before, size, -1, *after), dim, 0)


def sum_at_owner(value, axis, dim):
    size = lax.axis_size(axis)
    parts = lax.all_to_all(split_up(value, dim, size), axis, 0, 0, tiled=True)
    return jnp.sum(parts, axis=0)


def sent_to_all(value, axis):
    copies = jnp.broadcast_to(value, (lax.axis_size(axis), *value.shape))
    return lax.all_to_all(copies, axis, split_axis=0, concat_axis=0, tiled=True)


def of_everyone(value, axis):
    return sent_to_all(value, axis).sum(axis=0)


def split_heads(array, block_len, width):
    length = array.shape[0]
    return array.reshape(length // block_len, block_len, -1, width).transpose(2, 0, 1, 3)


def merge_heads(array):
    return array.transpose(1, 2, 0, 3).reshape(array.shape[1] * array.shape[2], -1)


def narrow_product(form, left, right):
    return jnp.einsum(form, left, right, preferred_element_type=jnp.float32)


def state_product(form, left, right):
    return jnp.einsum(form, left.astype(jnp.float32), right)


def carry_combine(earlier, later):
    return (earlier[0] * later[0], later[0][..., None] * earlier[1] + later[1])


def on_device(block_input, queries, keys, w_value, log_decay, d_out):
    q_scale = DK ** (-0.5)
    block_len = 32
    values = jnp.dot(block_input, w_value, preferred_element_type=jnp.float32).astype(jnp.bfloat16)
    q_heads = split_heads(queries, block_len, DK).astype(jnp.float32) * q_scale
    k_heads = split_heads(keys, block_len, DK).astype(jnp.float32)
    v_heads = split_heads(values, block_len, DV)
    g_heads = split_heads(log_decay, block_len, DK)
    o_grad = split_heads(d_out, block_len, DV)
    cumlog = jnp.cumsum(g_heads, axis=2)
    last_log = cumlog[:, :, -1, :]
    last_wide = last_log[:, :, None, :]
    log_total = jnp.sum(last_log, axis=1)
    span_decay = jnp.exp(log_total)
    block_decay = jnp.exp(last_log)
    before_log = jnp.cumsum(last_log, axis=1) - last_log
    after_log = log_total[:, None, :] - jnp.cumsum(last_log, axis=1)
    k_tail = jnp.exp(last_wide - cumlog)
    q_grown = (q_heads * jnp.exp(cumlog)).astype(jnp.bfloat16)
    k_shrunk = (k_heads * jnp.exp(-cumlog)).astype(jnp.bfloat16)
    k_tailed = (k_heads * k_tail).astype(jnp.bfloat16)
    increments = narrow_product("hbcd,hbcv->hbdv", k_tailed, v_heads)
    backwards = narrow_product("hbcd,hbcv->hbdv", q_grown, o_grad)

    def forward_step(carried, inputs):
        decay_block, grown = inputs
        return (decay_block[:, :, None] * carried + grown, carried)

    def backward_step(adjoint, inputs):
        decay_block, grown = inputs
        return (grown + decay_block[:, :, None] * adjoint, adjoint)

    zero_state = jnp.zeros_like(increments[:, 0])
    span_state, local_states = lax.scan(
        forward_step, zero_state, (jnp.moveaxis(block_decay, 1, 0), jnp.moveaxis(increments, 1, 0))
    )
    span_adjoint, local_adjoints = lax.scan(
        backward_step,
        zero_state,
        (jnp.moveaxis(block_decay, 1, 0), jnp.moveaxis(backwards, 1, 0)),
        reverse=True,
    )
    identity = (jnp.ones_like(span_decay), jnp.zeros_like(span_state))
    _, state_in = prefix_by_axis((span_decay, span_state), SP, carry_combine, identity, False)
    _, adjoint_in = prefix_by_axis((span_decay, span_adjoint), SP, carry_combine, identity, True)
    entering = jnp.moveaxis(local_states, 0, 1) + jnp.exp(before_log)[..., None] * state_in[:, None]
    from_right = (
        jnp.moveaxis(local_adjoints, 0, 1) + jnp.exp(after_log)[..., None] * adjoint_in[:, None]
    )
    span_end = span_state + span_decay[..., None] * state_in
    decay_carry = jnp.sum(adjoint_in * span_end, axis=-1)
    causal = jnp.tril(jnp.ones((block_len, block_len), jnp.float32))
    out_dots = (narrow_product("hbcv,hbsv->hbcs", o_grad, v_heads) * causal).astype(jnp.bfloat16)
    key_dots = (narrow_product("hbcd,hbsd->hbcs", q_grown, k_shrunk) * causal).astype(jnp.bfloat16)
    q_adjoint = jnp.exp(cumlog) * (
        state_product("hbcv,hbdv->hbcd", o_grad, entering)
        + narrow_product("hbcs,hbsd->hbcd", out_dots, k_shrunk)
    )
    k_grad = jnp.exp(-cumlog) * narrow_product(
        "hbcs,hbcd->hbsd", out_dots, q_grown
    ) + k_tail * state_product("hbsv,hbdv->hbsd", v_heads, from_right)
    v_grad = narrow_product("hbcs,hbcv->hbsv", key_dots, o_grad) + state_product(
        "hbsd,hbdv->hbsv", k_tailed, from_right
    )
    decay_terms = merge_heads(q_heads * q_adjoint - k_heads * k_grad)
    d_log_decay = (
        jnp.flip(jnp.cumsum(jnp.flip(decay_terms, 0), 0), 0) + decay_carry.reshape(-1)[None, :]
    )
    value_grad = merge_heads(v_grad).astype(jnp.bfloat16)
    d_w_value = sum_at_owner(
        lax.dot_general(
            block_input, value_grad, (((0,), (0,)), ((), ())), preferred_element_type=jnp.float32
        ),
        SP,
        0,
    )
    row_norms = of_everyone(jnp.sum(d_w_value * d_w_value, axis=1), "tp")
    d_queries = merge_heads(q_adjoint * q_scale).astype(jnp.bfloat16)
    d_keys = merge_heads(k_grad).astype(jnp.bfloat16)
    return (d_queries, d_keys, d_log_decay, d_w_value, row_norms)


def solution(mesh):
    torus = Mesh(mesh.devices.reshape(8, 4, mesh.shape["tp"]), ("sp_0", "sp_1", "tp"))
    in_specs = (P(SP, None), P(SP, "tp"), P(SP, "tp"), P(None, "tp"), P(SP, "tp"), P(SP, "tp"))
    out_specs = (P(SP, "tp"), P(SP, "tp"), P(SP, "tp"), P(SP, "tp"), P(SP))
    return jax.shard_map(
        on_device, mesh=torus, in_specs=in_specs, out_specs=out_specs, check_vma=False
    )
```

profile of v0, /device:TPU:1, one launch (start us, length us, event | category | flops | bytes accessed | tf_op | source)
XLA Modules:
  0.0 221.2 jit_solution(9497038292571211023)
XLA Ops:
  7.3 0.9 convert_multiply_fusion.3
  8.2 1.0 fusion.33
  9.3 1.7 convolution_convert_fusion
  11.1 1.3 convolution_bitcast_fusion.2
  12.5 8.5 %while.30 = (s32[]{:T(128)}, f32[1,128,256]{2,1,0:T(8,128)S(1)}, f32[8,1,128,256]{3,2,1,0:T(8,128)S(1)}, f32[8,1,128]{2,1,0:T(1,128)S(1)}, f32[8,1,128,256]{3,2,1,0:T(8,128)}, /*index=5*/s32[]{:T(128)}, s32[]{:T(128)}) while((s32[]{:T(128)}, f32[1,128,256]{2,1,0:T(8,128)S(1)}, f32[8,1,128,256]{3,2,1,0:T(8,128)S(1)}, ...), condition=%wide.region_2.3_spmd.clone, body=%wide.region_1.2_spmd.clone.sunk | while | flops 131075 | bytes 657004 | solution.py:107
  12.6 1.0 bitcast_add_fusion.33
  13.6 1.0 bitcast_add_fusion.33
  14.7 1.0 bitcast_add_fusion.33
  15.8 1.0 bitcast_add_fusion.33
  16.8 1.0 bitcast_add_fusion.33
  17.9 1.0 bitcast_add_fusion.33
  19.0 1.0 bitcast_add_fusion.33
  20.0 1.0 bitcast_add_fusion.33
  21.1 1.0 copy-done.1
  22.0 1.3 convolution_bitcast_fusion.1
  23.5 8.5 %while.31 = (s32[]{:T(128)}, f32[1,128,256]{2,1,0:T(8,128)S(1)}, f32[8,1,128,256]{3,2,1,0:T(8,128)S(1)}, f32[8,1,128,256]{3,2,1,0:T(8,128)}, f32[8,1,128]{2,1,0:T(1,128)S(1)}, /*index=5*/s32[]{:T(128)}, s32[]{:T(128)}, s32[]{:T(128)}) while((s32[]{:T(128)}, f32[1,128,256]{2,1,0:T(8,128)S(1)}, f32[8,1,128,256]{3,2,1,0:T(8,128)S(1)}, ...), condition=%wide.region_6.7_spmd.clone, body=%wide.region_5.6_spmd.clone.sunk | while | flops 131076 | bytes 657024 | solution.py:110
  23.5 1.0 bitcast_add_fusion.34
  24.6 1.0 bitcast_add_fusion.34
  25.7 1.0 bitcast_add_fusion.34
  26.7 1.0 bitcast_add_fusion.34
  27.8 1.0 bitcast_add_fusion.34
  28.9 1.0 bitcast_add_fusion.34
  29.9 1.0 bitcast_add_fusion.34
  31.0 1.0 bitcast_add_fusion.34
  32.0 12.3 %all-gather.2 = f32[4,128,256]{2,1,0:T(8,128)S(1)} all-gather(f32[1,128,256]{2,1,0:T(8,128)S(1)} %get-tuple-element.140), channel_id=4, replica_groups=mesh['sp_0'=8,'sp_1'=4,'tp'=8] {'sp_1'}, dimensions={0}, use_global_device_ids=true | all-gather | bytes 655360 | tf_op jit(solution)/shard_map/all_gather | solution.py:23
  44.8 7.1 %all-gather.3 = f32[4,1,128]{2,1,0:T(1,128)S(1)} all-gather(f32[1,1,128]{2,1,0:T(1,128)S(1)} %get-tuple-element.286), channel_id=2, replica_groups=mesh['sp_0'=8,'sp_1'=4,'tp'=8] {'sp_1'}, dimensions={0}, use_global_device_ids=true | all-gather | bytes 2560 | tf_op jit(solution)/shard_map/all_gather | solution.py:23
  52.5 9.9 %all-gather.1 = f32[4,128,256]{2,1,0:T(8,128)S(1)} all-gather(f32[1,128,256]{2,1,0:T(8,128)S(1)} %get-tuple-element.138), channel_id=3, replica_groups=mesh['sp_0'=8,'sp_1'=4,'tp'=8] {'sp_1'}, dimensions={0}, use_global_device_ids=true | all-gather | bytes 655360 | tf_op jit(solution)/shard_map/all_gather | solution.py:23
  63.0 0.9 bitcast_add_fusion.23
  64.6 14.6 %all_gather.39 = f32[8,1,128]{2,1,0:T(1,128)S(1)} all-gather(f32[1,1,128]{2,1,0:T(1,128)S(1)} %get-tuple-element.277), channel_id=1, replica_groups=mesh['sp_0'=8,'sp_1'=4,'tp'=8] {'sp_0'}, dimensions={0}, use_global_device_ids=true | all-gather | bytes 4608 | tf_op jit(solution)/shard_map/all_gather | solution.py:23
  79.8 1.3 subtract_exponential_fusion
  81.1 25.2 %all-gather.9.cloned.1.call-done = f32[8,1,128,256]{3,2,1,0:T(8,128)} async-done(((f32[1,1,128,256]{3,2,1,0:T(8,128)}), f32[8,1,128,256]{3,2,1,0:T(8,128)}) %all-gather.9.cloned.1.call-update) | async-done | bytes 1048592 | tf_op jit(solution)/shard_map/all_gather | solution.py:23
  106.3 1.6 add_bitcast_fusion
  108.5 1.9 fusion.9
  110.4 2.0 fusion.2
  112.5 2.7 %convolution_bitcast_fusion = f32[2048,256]{0,1:T(8,128)} fusion(bf16[256,256]{1,0:T(8,128)(2,1)} %bitcast.332, bf16[256,2048]{1,0:T(8,128)(2,1)S(1)} %copy-done), kind=kOutput, calls=%fused_computation.8 | convolution fusion | flops 268435456 | bytes 3276800 | tf_op jit(solution)/shard_map/dot_general | solution.py:144
  115.1 2.9 %copy.60 = f32[2048,256]{1,0:T(8,128)} copy(f32[2048,256]{0,1:T(8,128)} %convolution_bitcast_fusion) | data formatting | bytes 4194304 | tf_op jit(solution)/shard_map/dot_general | solution.py:144
  118.0 7.4 %all-to-all-start = ((f32[32,64,256]{2,1,0:T(8,128)}), f32[32,64,256]{2,1,0:T(8,128)}, u32[]{:S(2)}, u32[]{:S(2)}) async-start(f32[32,64,256]{2,1,0:T(8,128)} %bitcast.317), calls=%async_computation | async-start | bytes 4194304 | tf_op jit(solution)/shard_map/all_to_all | solution.py:40
  125.5 0.7 all-gather.7.cloned.1.call-update
  126.2 56.7 %all_gather.35 = f32[8,1,128]{2,1,0:T(1,128)S(1)} all-gather(f32[1,1,128]{2,1,0:T(1,128)} %get-tuple-element.278), channel_id=1, replica_groups=mesh['sp_0'=8,'sp_1'=4,'tp'=8] {'sp_0'}, dimensions={0}, use_global_device_ids=true | all-gather | bytes 4608 | tf_op jit(solution)/shard_map/all_gather | solution.py:23
  183.5 1.7 fusion.6
  185.3 1.7 add_bitcast_fusion.1
  187.0 1.3 convolution_bitcast_fusion.4
  189.0 0.8 fusion.18
  190.2 2.3 %fusion.25 = f32[128]{0:T(128)S(1)} fusion(f32[1,128,256]{2,1,0:T(8,128)S(1)} %get-tuple-element.138, f32[8,1,128,256]{3,2,1,0:T(8,128)} %all-gather.9.cloned.1.call-done, f32[4,128,256]{2,1,0:T(8,128)S(1)} %all-gather.2, f32[8,1,128,256]{3,2,1,0:T(8,128)} %all-gather.7.cloned.1.call-done, f32[4,128,256]{2,1,0:T(8,128)S(1)} %all-gather.1, f32[128]{0:T(128)} %copy-done.23, ...), kind=kLoop, calls=%fused_computation.48 | loop fusion | flops 2490240 | bytes 3290136 | tf_op jit(solution)/shard_map/reduce_sum | solution.py:124
  192.5 1.7 reduce_sum.47
  194.9 14.3 %all-to-all-start.1 = ((f32[8,1,64]{2,1,0:T(1,128)}), f32[8,1,64]{2,1,0:T(1,128)S(1)}, u32[]{:S(2)}, u32[]{:S(2)}) async-start(f32[8,1,64]{2,1,0:T(1,128)} %broadcast_in_dim.41), calls=%async_computation.1 | async-start | bytes 8192 | tf_op jit(solution)/shard_map/all_to_all | solution.py:46
  209.3 0.7 broadcast_add_fusion
  209.9 3.9 %all-to-all-done.1 = f32[8,1,64]{2,1,0:T(1,128)S(1)} async-done(((f32[8,1,64]{2,1,0:T(1,128)}), f32[8,1,64]{2,1,0:T(1,128)S(1)}, u32[]{:S(2)}, u32[]{:S(2)}) %all-to-all-start.1) | async-done | bytes 2080 | tf_op jit(solution)/shard_map/all_to_all | solution.py:46
  (117 shorter events, 7.2 us)
Async XLA Ops:
  7.2 2.1 copy-start
  7.2 3.8 %copy-start.10 = (bf16[256,128]{1,0:T(8,128)(2,1)S(1)}, bf16[256,128]{1,0:T(8,128)(2,1)}, u32[]{:S(2)}) copy-start(bf16[256,128]{1,0:T(8,128)(2,1)} %param.12) | copy-start | bytes 196612
  7.2 99.1 %all-gather.9.cloned.1.call-start = ((), (), s32[]{:S(2)}) async-start(), calls=%async_computation.3 | async-start | bytes 1179648 | tf_op jit(solution)/shard_map/all_gather | solution.py:23
  8.2 4.2 %copy-start.4 = (f32[256,128]{1,0:T(8,128)}, f32[256,128]{1,0:T(8,128)S(1)}, u32[]{:S(2)}) copy-start(f32[256,128]{1,0:T(8,128)S(1)} %convert_multiply_fusion.3) | copy-start | bytes 393220
  9.3 35.0 %copy-start.26 = (f32[128]{0:T(128)}, f32[128]{0:T(128)S(1)}, u32[]{:S(2)}) copy-start(f32[128]{0:T(128)S(1)} %get-tuple-element.252) | copy-start | bytes 1540
  9.3 54.7 %copy-start.15 = (f32[8,128]{1,0:T(8,128)}, f32[8,128]{1,0:T(8,128)S(1)}, u32[]{:S(2)}) copy-start(f32[8,128]{1,0:T(8,128)S(1)} %get-tuple-element.253) | copy-start | bytes 12292
  11.0 1.5 copy-start.12
  11.1 10.0 %copy-start.8 = (bf16[8,32,128]{2,1,0:T(8,128)(2,1)}, bf16[8,32,128]{2,1,0:T(8,128)(2,1)S(1)}, u32[]{:S(2)}) copy-start(bf16[8,32,128]{2,1,0:T(8,128)(2,1)S(1)} %get-tuple-element.250) | copy-start | bytes 196612
  12.4 9.6 %copy-start.3 = (bf16[256,256]{1,0:T(8,128)(2,1)S(1)}, bf16[256,256]{1,0:T(8,128)(2,1)}, u32[]{:S(2)}) copy-start(bf16[256,256]{1,0:T(8,128)(2,1)} %param.15) | copy-start | bytes 393220
  21.0 1.0 copy-start.1
  52.5 10.5 %copy-start.18 = (f32[128]{0:T(128)}, f32[128]{0:T(128)S(1)}, u32[]{:S(2)}) copy-start(f32[128]{0:T(128)S(1)} %get-tuple-element.279) | copy-start | bytes 1540
  52.5 11.4 %copy-start.20 = (f32[128]{0:T(128)}, f32[128]{0:T(128)S(1)}, u32[]{:S(2)}) copy-start(f32[128]{0:T(128)S(1)} %get-tuple-element.280) | copy-start | bytes 1540
  52.5 11.4 %copy-start.24 = (f32[128]{0:T(128)}, f32[128]{0:T(128)S(1)}, u32[]{:S(2)}) copy-start(f32[128]{0:T(128)S(1)} %get-tuple-element.281) | copy-start | bytes 1540
  52.5 11.4 %copy-start.25 = (f32[128]{0:T(128)}, f32[128]{0:T(128)S(1)}, u32[]{:S(2)}) copy-start(f32[128]{0:T(128)S(1)} %get-tuple-element.282) | copy-start | bytes 1540
  63.0 0.9 copy-start.22
  63.0 0.9 copy-start.23
  107.9 0.6 copy-start.6
  118.0 74.4 %all-to-all-start = ((f32[32,64,256]{2,1,0:T(8,128)}), f32[32,64,256]{2,1,0:T(8,128)}, u32[]{:S(2)}, u32[]{:S(2)}) async-start(f32[32,64,256]{2,1,0:T(8,128)} %bitcast.317), calls=%async_computation | async-start | bytes 4194304 | tf_op jit(solution)/shard_map/all_to_all | solution.py:40
  125.4 59.8 %all-gather.7.cloned.1.call-start = ((), (), s32[]{:S(2)}) async-start(), calls=%async_computation.2 | async-start | bytes 1179648 | tf_op jit(solution)/shard_map/all_gather | solution.py:23
  185.2 3.3 %copy-start.16 = (f32[8,128]{1,0:T(8,128)S(1)}, f32[8,128]{1,0:T(8,128)}, u32[]{:S(2)}) copy-start(f32[8,128]{1,0:T(8,128)} %copy-done.15) | copy-start | bytes 12292
  185.2 3.4 %copy-start.17 = (f32[8,128]{1,0:T(8,128)S(1)}, f32[8,128]{1,0:T(8,128)}, u32[]{:S(2)}) copy-start(f32[8,128]{1,0:T(8,128)} %get-tuple-element.255) | copy-start | bytes 12292
  185.2 1.8 copy-start.2
  185.2 3.1 %copy-start.11 = (bf16[256,128]{1,0:T(8,128)(2,1)S(1)}, bf16[256,128]{1,0:T(8,128)(2,1)}, u32[]{:S(2)}) copy-start(bf16[256,128]{1,0:T(8,128)(2,1)} %param.12) | copy-start | bytes 196612
  185.2 3.1 %copy-start.13 = (bf16[8,32,32]{1,2,0:T(8,128)(2,1)S(1)}, bf16[8,32,32]{1,2,0:T(8,128)(2,1)}, u32[]{:S(2)}) copy-start(bf16[8,32,32]{1,2,0:T(8,128)(2,1)} %fusion.6) | copy-start | bytes 49156
  185.2 3.3 %copy-start.7 = (f32[128,256]{1,0:T(8,128)S(1)}, f32[128,256]{1,0:T(8,128)}, u32[]{:S(2)}) copy-start(f32[128,256]{1,0:T(8,128)} %copy-done.6) | copy-start | bytes 393220
  187.0 2.0 copy-start.5
  187.0 2.0 copy-start.9
  188.3 1.8 copy-start.19
  188.3 1.8 copy-start.21
  194.2 20.2 %copy-start.14 = (f32[64,256]{1,0:T(8,128)}, f32[64,256]{1,0:T(8,128)S(1)}, u32[]{:S(2)}) copy-start(f32[64,256]{1,0:T(8,128)S(1)} %reduce_sum.47) | copy-start | bytes 196612
  194.9 18.9 %all-to-all-start.1 = ((f32[8,1,64]{2,1,0:T(1,128)}), f32[8,1,64]{2,1,0:T(1,128)S(1)}, u32[]{:S(2)}, u32[]{:S(2)}) async-start(f32[8,1,64]{2,1,0:T(1,128)} %broadcast_in_dim.41), calls=%async_computation.1 | async-start | bytes 8192 | tf_op jit(solution)/shard_map/all_to_all | solution.py:46
Sparse Core Ops, SparseCore 0:
  64.1 42.1 all-gather.8
  128.0 53.5 all-gather.6
where the time goes:
time: 222 us; the launch traced here: 221 us
  blocking collectives  101 us (45%)
  other arithmetic  32.3 us (15%)
  waiting for transfers between devices  29.9 us (13%)
  starting transfers between devices  21.8 us (10%)
  matrix products  15.3 us (7%)
  between operations  14.5 us (7%)
  local copies, waits for them, and re-layouts  6.23 us (3%)
    all_gather x5, blocking collectives, prefix_by_axis(): pieces = jax.tree.map(lambda part: lax.all_gather(part, axis), subtotal)  101 us
    all_gather x2, waiting for transfers between devices, prefix_by_axis(): pieces = jax.tree.map(lambda part: lax.all_gather(part, axis), subtotal)  25.2 us
    all_to_all x1, starting transfers between devices, sent_to_all(): return lax.all_to_all(copies, axis, split_axis=0, concat_axis=0, tiled=True)  14.3 us
    add x8, other arithmetic, forward_step(): return (decay_block[:, :, None] * carried + grown, carried)  8 us
    add x8, other arithmetic, backward_step(): return (grown + decay_block[:, :, None] * adjoint, adjoint)  8 us
    dot_general x6, matrix products, narrow_product(): return jnp.einsum(form, left, right, preferred_element_type=jnp.float32)  7.44 us
    all_to_all x1, starting transfers between devices, sum_at_owner(): parts = lax.all_to_all(split_up(value, dim, size), axis, 0, 0, tiled=True)  7.39 us
  transfers between devices with their start and end apart: 4, of which 2 were waited for; matrix products, arithmetic and copies ran while one was open for 6% of the time, Pallas kernels for 0%

commit v1 on v0

v1 whole, which is shorter than its diff:
```python
import jax
import jax.numpy as jnp
from jax import lax
from jax.experimental import pallas as pl
from jax.experimental.pallas import tpu as pltpu
from jax.sharding import PartitionSpec as P

DK = 128
DV = 256
T = 256
BLK = 32
NB = T // BLK
NZ, NX, NT = 8, 4, 8
SLAB = DV // NX
ROWS = 64
MESH = pl.DeviceIdType.MESH
F32, BF16 = jnp.float32, jnp.bfloat16


def dot(a, b):
    return jnp.dot(a, b, preferred_element_type=F32)


def dot_nt(a, b):
    return lax.dot_general(a, b, (((1,), (1,)), ((), ())), preferred_element_type=F32)


def dot_tn(a, b):
    return lax.dot_general(a, b, (((0,), (0,)), ((), ())), preferred_element_type=F32)


def exact_sum(ones, a):
    hi = a.astype(BF16)
    rest = a - hi.astype(F32)
    mid = rest.astype(BF16)
    low = (rest - mid.astype(F32)).astype(BF16)
    return dot(ones, hi) + (dot(ones, mid) + dot(ones, low))


def kernel(
    x_hbm, q_hbm, k_hbm, w_hbm, g_hbm, do_hbm,
    dq_hbm, dk_hbm, dg_hbm, dw_hbm, rn_hbm,
    x_v, q_v, k_v, w_v, g_v, do_v, dq_v, dk_v, dg_v, dwo_v, rn_v,
    xt_v, val_v, locs_v, adjs_v,
    x1s, x1r, z2s, z2r, x3s, x3r, dwp, rxr, rxs, rzr, tps, tpr,
    in_sem, out_sem, x1_ss, x1_rs, z2_ss, z2_rs, x3_ss, x3_rs, rx_ss, rx_rs, rz_ss, rz_rs, tp_ss, tp_rs,
):
    sp, tp = lax.axis_index("sp"), lax.axis_index("tp")
    z, x = sp // NX, lax.rem(sp, NX)

    def x_dev(t):
        return {"sp": z * NX + t}

    def z_dev(t):
        return {"sp": t * NX + x}

    def tp_dev(t):
        return {"tp": t}

    barrier = pltpu.get_barrier_semaphore()
    for k in range(1, NX):
        pl.semaphore_signal(barrier, inc=1, device_id=x_dev(lax.rem(x + k, NX)), device_id_type=MESH)
    for k in range(1, NZ):
        pl.semaphore_signal(barrier, inc=1, device_id=z_dev(lax.rem(z + k, NZ)), device_id_type=MESH)
    for k in range(1, NT):
        pl.semaphore_signal(barrier, inc=1, device_id=tp_dev(lax.rem(tp + k, NT)), device_id_type=MESH)

    loads = [
        pltpu.make_async_copy(src, dst, in_sem.at[i])
        for i, (src, dst) in enumerate(
            ((g_hbm, g_v), (q_hbm, q_v), (do_hbm, do_v), (k_hbm, k_v), (x_hbm, x_v), (w_hbm, w_v))
        )
    ]
    for load in loads:
        load.start()

    def remote(src, dst, ss, rs, dev):
        return pltpu.make_async_remote_copy(
            src_ref=src, dst_ref=dst, send_sem=ss, recv_sem=rs, device_id=dev, device_id_type=MESH
        )

    row = lax.broadcasted_iota(jnp.int32, (T, T), 0)
    col = lax.broadcasted_iota(jnp.int32, (T, T), 1)
    same = (row >> 5) == (col >> 5)
    lower = same & (col <= row)
    upper = same & (col >= row)

    loads[0].wait()
    c = exact_sum(lower.astype(BF16), g_v[...])
    c3 = c.reshape(NB, BLK, DK)
    ends = [c3[b, BLK - 1 : BLK, :] for b in range(NB)]
    before = [jnp.zeros((1, DK), F32)]
    for b in range(NB):
        before.append(before[-1] + ends[b])
    after = [jnp.zeros((1, DK), F32)]
    for b in reversed(range(1, NB)):
        after.append(after[-1] + ends[b])
    after = after[::-1]
    total = before[NB]

    def per_block(rows):
        return jnp.concatenate([jnp.broadcast_to(r, (BLK, DK)) for r in rows], axis=0)

    end_wide = per_block(ends)
    from_start = jnp.exp(c + per_block(before[:NB]))
    tail_log = end_wide - c
    to_end = jnp.exp(tail_log + per_block(after))
    span_decay = jnp.exp(total)

    loads[1].wait()
    loads[2].wait()
    qs = q_v[...].astype(F32) * (DK**-0.5)
    do = do_v[...]
    span_adj = dot_tn(do, (qs * from_start).astype(BF16))
    wide_decay = jnp.broadcast_to(span_decay, (8, DK))
    for s in range(NX):
        x1s[0, s, :SLAB, :] = span_adj[s * SLAB : (s + 1) * SLAB]
        x1s[0, s, SLAB:, :] = wide_decay
    pl.semaphore_wait(barrier, NX - 1 + NZ - 1 + NT - 1)

    started = []

    def x_leg(i):
        for k in (2, 1, 3):
            t = lax.rem(x + k, NX)
            cp = remote(x1s.at[i, t], x1r.at[i, x], x1_ss.at[i, k], x1_rs.at[i, k], x_dev(t))
            cp.start()
            started.append(cp)
        x1r[i, x] = x1s[i, x]

    def x_leg_wait(i):
        for k in (2, 1, 3):
            t = lax.rem(x + NX - k, NX)
            remote(x1s.at[i, t], x1r.at[i, t], x1_ss.at[i, k], x1_rs.at[i, k], x_dev(t)).wait_recv()

    x_leg(0)

    loads[3].wait()
    kf = k_v[...].astype(F32)
    k_end = (kf * to_end).astype(BF16)
    loads[4].wait()
    loads[5].wait()
    val_v[...] = dot(x_v[...], w_v[...]).astype(BF16)
    v = val_v[...]
    span_state = dot_tn(v, k_end)
    for s in range(NX):
        x1s[1, s, :SLAB, :] = span_state[s * SLAB : (s + 1) * SLAB]
        x1s[1, s, SLAB:, :] = wide_decay
    x_leg(1)

    def slab(i, t):
        return x1r[i, t, :SLAB, :]

    def slab_decay(i, t):
        return x1r[i, t, SLAB : SLAB + 1, :]

    def group_total(i, order):
        x_leg_wait(i)
        acc = slab(i, order[0])
        dec = slab_decay(i, order[0])
        for t in order[1:]:
            acc = slab(i, t) + slab_decay(i, t) * acc
            dec = dec * slab_decay(i, t)
        z2s[i, :SLAB, :] = acc
        z2s[i, SLAB:, :] = jnp.broadcast_to(dec, (8, DK))

    def z_copy(i, k, t, slot):
        return remote(z2s.at[i], z2r.at[i, slot], z2_ss.at[i, k], z2_rs.at[i, k], z_dev(t))

    group_total(0, (3, 2, 1, 0))
    for k in (4, 3, 5, 2, 6, 1, 7):
        @pl.when(z >= k)
        def _():
            z_copy(0, k, z - k, z).start()

    group_total(1, (0, 1, 2, 3))
    for k in (4, 3, 5, 2, 6, 1, 7):
        @pl.when(z + k < NZ)
        def _():
            z_copy(1, k, z + k, z).start()

    exp_c = jnp.exp(c)
    exp_nc = jnp.exp(-c)
    exp_tail = jnp.exp(tail_log)
    grown_q = (qs * exp_c).astype(BF16)
    shrunk_k = (kf * exp_nc).astype(BF16)
    tail_k = (kf * exp_tail).astype(BF16)
    adj = jnp.zeros((DV, DK), F32)
    for b in reversed(range(NB)):
        sl = slice(b * BLK, (b + 1) * BLK)
        adjs_v[b] = adj.astype(BF16)
        if b:
            adj = jnp.exp(ends[b]) * adj + dot_tn(do[sl], grown_q[sl])
    key_dots_t = jnp.where(upper, dot_nt(shrunk_k, grown_q), 0.0).astype(BF16)
    local_vg = dot(key_dots_t, do) + jnp.concatenate(
        [dot_nt(tail_k[b * BLK : (b + 1) * BLK], adjs_v[b]) for b in range(NB)], axis=0
    )

    def enter(i, t, acc):
        x3s[i, t] = acc

    def x3_leg(i):
        for k in (2, 1, 3):
            t = lax.rem(x + k, NX)
            cp = remote(x3s.at[i, t], x3r.at[i, x], x3_ss.at[i, k], x3_rs.at[i, k], x_dev(t))
            cp.start()
            started.append(cp)
        x3r[i, x] = x3s[i, x]

    def x3_wait(i):
        for k in (2, 1, 3):
            t = lax.rem(x + NX - k, NX)
            remote(x3s.at[i, t], x3r.at[i, t], x3_ss.at[i, k], x3_rs.at[i, k], x_dev(t)).wait_recv()

    def adj_step(n, acc):
        t = NZ - 1 - n
        z_copy(0, t - z, t, t).wait_recv()
        return z2r[0, t, :SLAB, :] + z2r[0, t, SLAB : SLAB + 1, :] * acc

    acc = lax.fori_loop(0, NZ - 1 - z, adj_step, jnp.zeros((SLAB, DK), F32))
    for t in (3, 2, 1, 0):
        enter(0, t, acc)
        if t:
            acc = slab(0, t) + slab_decay(0, t) * acc
    x3_leg(0)

    def state_step(t, acc):
        z_copy(1, z - t, t, t).wait_recv()
        return z2r[1, t, :SLAB, :] + z2r[1, t, SLAB : SLAB + 1, :] * acc

    acc = lax.fori_loop(0, z, state_step, jnp.zeros((SLAB, DK), F32))
    for t in range(NX):
        enter(1, t, acc)
        if t < NX - 1:
            acc = slab(1, t) + slab_decay(1, t) * acc
    x3_leg(1)

    for zz in range(NZ):
        xt_v[:, zz] = x_v[:, zz * NX * ROWS : (zz + 1) * NX * ROWS].T.reshape(NX, ROWS, T)

    x3_wait(0)
    adj_in = x3r[0].reshape(DV, DK)
    adj_in16 = adj_in.astype(BF16)
    vg = (local_vg + dot_nt(k_end, adj_in16)).astype(BF16)
    for k in (2, 1, 3, 0):
        t = lax.rem(x + k, NX)
        part = dot(xt_v[t].reshape(NZ * ROWS, T), vg)
        for h in range(2):
            dwp[h, t] = part[:, h * 128 : (h + 1) * 128].reshape(NZ, ROWS, 128)
            if k:
                cp = remote(dwp.at[h, t], rxr.at[h, x], rx_ss.at[h, k], rx_rs.at[h, k], x_dev(t))
                cp.start()
                started.append(cp)

    state = jnp.zeros((DV, DK), F32)
    for b in range(NB):
        sl = slice(b * BLK, (b + 1) * BLK)
        locs_v[b] = state.astype(BF16)
        if b < NB - 1:
            state = jnp.exp(ends[b]) * state + dot_tn(v[sl], tail_k[sl])
    out_dots = jnp.where(lower, dot_nt(do, v), 0.0).astype(BF16)
    out_dots_t = jnp.where(upper, dot_nt(v, do), 0.0).astype(BF16)
    local_qg = dot(out_dots, shrunk_k) + jnp.concatenate(
        [dot(do[b * BLK : (b + 1) * BLK], locs_v[b]) for b in range(NB)], axis=0
    )
    local_kg = exp_nc * dot(out_dots_t, grown_q) + exp_tail * jnp.concatenate(
        [dot(v[b * BLK : (b + 1) * BLK], adjs_v[b]) for b in range(NB)], axis=0
    )
    kg = local_kg + to_end * dot(v, adj_in16)
    dk_v[...] = kg.astype(BF16)
    x3_wait(1)
    state_in = x3r[1].reshape(DV, DK)
    qg = exp_c * local_qg + from_start * dot(do, state_in.astype(BF16))
    dq_v[...] = (qg * (DK**-0.5)).astype(BF16)
    carry = jnp.sum(adj_in * (span_state + span_decay * state_in), axis=0, keepdims=True)
    dg_v[...] = exact_sum((col >= row).astype(BF16), qs * qg - kf * kg) + carry
    stores = [
        pltpu.make_async_copy(src, dst, out_sem.at[i])
        for i, (src, dst) in enumerate(((dq_v, dq_hbm), (dk_v, dk_hbm), (dg_v, dg_hbm), (dwo_v, dw_hbm), (rn_v, rn_hbm)))
    ]
    for store in stores[:3]:
        store.start()

    for h in range(2):
        for k in (2, 1, 3):
            t = lax.rem(x + NX - k, NX)
            remote(dwp.at[h, t], rxr.at[h, t], rx_ss.at[h, k], rx_rs.at[h, k], x_dev(t)).wait_recv()
        for k in (4, 3, 5, 2, 6, 1, 7, 0):
            t = lax.rem(z + k, NZ)
            piece = dwp[h, x, t]
            for j in range(1, NX):
                piece = piece + rxr[h, lax.rem(x + j, NX), t]
            rxs[h, t] = piece
            if k:
                cp = remote(rxs.at[h, t], rzr.at[h, z], rz_ss.at[h, k], rz_rs.at[h, k], z_dev(t))
                cp.start()
                started.append(cp)
    squares = jnp.zeros((ROWS, 128), F32)
    for h in range(2):
        piece = rxs[h, z]
        for k in (1, 7, 2, 6, 3, 5, 4):
            t = lax.rem(z + NZ - k, NZ)
            remote(rxs.at[h, t], rzr.at[h, t], rz_ss.at[h, k], rz_rs.at[h, k], z_dev(t)).wait_recv()
            piece = piece + rzr[h, t]
        dwo_v[:, h * 128 : (h + 1) * 128] = piece
        squares = squares + piece * piece
    stores[3].start()

    norms = jnp.sum(squares.T, axis=0, keepdims=True)
    tps[...] = jnp.broadcast_to(jnp.concatenate([norms, jnp.zeros((1, 64), F32)], axis=1), (8, 128))
    for k in range(1, NT):
        t = lax.rem(tp + k, NT)
        cp = remote(tps, tpr.at[tp], tp_ss.at[k], tp_rs.at[k], tp_dev(t))
        cp.start()
        started.append(cp)
    acc = tps[0:1, :]
    for k in range(1, NT):
        t = lax.rem(tp + NT - k, NT)
        remote(tps, tpr.at[t], tp_ss.at[k], tp_rs.at[k], tp_dev(t)).wait_recv()
        acc = acc + tpr[t, 0:1, :]
    rn_v[...] = acc[:, :ROWS]
    stores[4].start()

    for cp in started:
        cp.wait_send()
    for k in range(1, NZ):
        @pl.when(z >= k)
        def _():
            z_copy(0, k, z - k, z).wait_send()

        @pl.when(z + k < NZ)
        def _():
            z_copy(1, k, z + k, z).wait_send()
    for store in stores:
        store.wait()


def on_device(block_input, queries, keys, w_value, log_decay, d_out):
    any_spec = pl.BlockSpec(memory_space=pl.ANY)
    dma = pltpu.SemaphoreType.DMA
    outs = pl.pallas_call(
        kernel,
        out_shape=(
            jax.ShapeDtypeStruct((T, DK), BF16),
            jax.ShapeDtypeStruct((T, DK), BF16),
            jax.ShapeDtypeStruct((T, DK), F32),
            jax.ShapeDtypeStruct((ROWS, DV), F32),
            jax.ShapeDtypeStruct((1, ROWS), F32),
        ),
        in_specs=[any_spec] * 6,
        out_specs=(any_spec,) * 5,
        scratch_shapes=[
            pltpu.VMEM((T, 2048), BF16), pltpu.VMEM((T, DK), BF16), pltpu.VMEM((T, DK), BF16),
            pltpu.VMEM((2048, DV), BF16), pltpu.VMEM((T, DK), F32), pltpu.VMEM((T, DV), BF16),
            pltpu.VMEM((T, DK), BF16), pltpu.VMEM((T, DK), BF16), pltpu.VMEM((T, DK), F32),
            pltpu.VMEM((ROWS, DV), F32), pltpu.VMEM((1, ROWS), F32),
            pltpu.VMEM((NX, NZ, ROWS, T), BF16), pltpu.VMEM((T, DV), BF16),
            pltpu.VMEM((NB, DV, DK), BF16), pltpu.VMEM((NB, DV, DK), BF16),
            pltpu.VMEM((2, NX, SLAB + 8, DK), F32), pltpu.VMEM((2, NX, SLAB + 8, DK), F32),
            pltpu.VMEM((2, SLAB + 8, DK), F32), pltpu.VMEM((2, NZ, SLAB + 8, DK), F32),
            pltpu.VMEM((2, NX, SLAB, DK), F32), pltpu.VMEM((2, NX, SLAB, DK), F32),
            pltpu.VMEM((2, NX, NZ, ROWS, 128), F32), pltpu.VMEM((2, NX, NZ, ROWS, 128), F32),
            pltpu.VMEM((2, NZ, ROWS, 128), F32), pltpu.VMEM((2, NZ, ROWS, 128), F32),
            pltpu.VMEM((8, 128), F32), pltpu.VMEM((NT, 8, 128), F32),
            dma((6,)), dma((5,)), dma((2, NX)), dma((2, NX)), dma((2, NZ)), dma((2, NZ)),
            dma((2, NX)), dma((2, NX)), dma((2, NX)), dma((2, NX)), dma((2, NZ)), dma((2, NZ)),
            dma((NT,)), dma((NT,)),
        ],
        compiler_params=pltpu.CompilerParams(collective_id=0, has_side_effects=True),
        name="gla_backward",
    )(block_input, queries, keys, w_value, log_decay, d_out)
    return (*outs[:4], outs[4].reshape(ROWS))


def solution(mesh):
    in_specs = (P("sp", None), P("sp", "tp"), P("sp", "tp"), P(None, "tp"), P("sp", "tp"), P("sp", "tp"))
    out_specs = (P("sp", "tp"), P("sp", "tp"), P("sp", "tp"), P("sp", "tp"), P("sp"))
    return jax.shard_map(on_device, mesh=mesh, in_specs=in_specs, out_specs=out_specs, check_vma=False)
```

time: 222 us -> 66.7 us (0.30)
  blocking collectives: 101 us -> 0 us
  Pallas kernels: 0 us -> 61.7 us
  other arithmetic: 32.3 us -> 0 us
  waiting for transfers between devices: 29.9 us -> 0 us
  starting transfers between devices: 21.8 us -> 0 us
  matrix products: 15.3 us -> 0 us
  between operations: 14.5 us -> 0.66 us
    all_gather x5 -> x0, blocking collectives: 101 us -> none  [prefix_by_axis(): pieces = jax.tree.map(lambda part: lax.all_gather(part, axis), subtotal)]
    pallas_call x0 -> x1, Pallas kernels: none -> 61.7 us  [on_device(): pl.pallas_call(kernel, out_shape=(jax.ShapeDtypeStruct((T, DK), BF16), ja...]
    all_gather x2 -> x0, waiting for transfers between devices: 25.2 us -> none  [prefix_by_axis(): pieces = jax.tree.map(lambda part: lax.all_gather(part, axis), subtotal)]
    all_to_all x2 -> x0, starting transfers between devices: 21.7 us -> none  [the longest x1 14.3 us: sent_to_all(): return lax.all_to_all(copies, axis, split_axis=0, concat_axis=0, tiled=True)]
    add x18 -> x0, other arithmetic: 17.5 us -> none  [the longest x8 8 us: forward_step(): return (decay_block[:, :, None] * carried + grown, carried)]
    dot_general x11 -> x0, matrix products: 15.3 us -> none  [the longest x6 7.44 us: narrow_product(): return jnp.einsum(form, left, right, preferred_element_type=jnp.float32)]
    mul x6 -> x0, other arithmetic: 6.01 us -> none  [the longest x3 1.79 us: carry_combine(): return (earlier[0] * later[0], later[0][..., None] * earlier[1] + later[1])]
    reduce_sum x5 -> x0, other arithmetic: 4.69 us -> none  [the longest x1 2.32 us: on_device(): decay_carry = jnp.sum(adjoint_in * span_end, axis=-1)]
  transfers between devices with their start and end apart: 4 -> 0, of which waited for: 2 -> 0; matrix products, arithmetic and copies ran while one was open for 6% -> 0% of each run, Pallas kernels for 0% -> 0%
where the time goes in v1:
time: 66.7 us; the launch traced here: 66.6 us
  Pallas kernels  61.7 us (93%)
  local copies, waits for them, and re-layouts  4.16 us (6%)
    pallas_call x1, Pallas kernels, on_device(): pl.pallas_call(kernel, out_shape=(jax.ShapeDtypeStruct((T, DK), BF16), ja...  61.7 us
    unnamed x13, local copies, waits for them, and re-layouts  4.16 us

profile of v1, /device:TPU:1, one launch (start us, length us, event | category | flops | bytes accessed | tf_op | source)
XLA Modules:
  0.0 66.6 jit_solution(5723883421261363205)
XLA Ops:
  0.6 61.7 %gla_backward.1 = (bf16[256,128]{1,0:T(8,128)(2,1)}, bf16[256,128]{1,0:T(8,128)(2,1)}, f32[256,128]{1,0:T(8,128)}, f32[64,256]{1,0:T(8,128)}, f32[1,64]{1,0:T(1,128)}) custom-call(bf16[256,2048]{1,0:T(8,128)(2,1)} %x_hbm.1, bf16[256,128]{1,0:T(8,128)(2,1)} %q_hbm.1, bf16[256,128]{1,0:T(8,128)(2,1)} %k_hbm.1, bf16[2048,256]{1,0:T(8,128)(2,1)} %w_hbm.1, ...), custom_call_target="tpu_custom_call" | custom-call | tf_op jit(solution)/shard_map/gla_backward/pallas_call | solution.py:341
  62.4 0.0 copy-start.2
  62.4 0.0 copy-start
  62.4 1.5 %copy.16 = bf16[256,128]{1,0:T(8,128)(2,1)} copy(bf16[256,128]{1,0:T(8,128)(2,1)} %get-tuple-element.20) | data formatting | bytes 131072
  63.9 0.0 copy-done.2
  63.9 0.6 copy.17
  64.6 0.0 copy-done
  64.6 0.0 copy-start.1
  64.6 0.7 copy.18
  65.2 0.2 copy-done.1
  65.4 0.0 copy-start.3
  65.4 0.6 copy.19
  66.0 0.0 copy-done.3
  66.1 0.5 copy.20
Async XLA Ops:
  62.4 1.5 %copy-start.2 = (bf16[256,128]{1,0:T(8,128)(2,1)S(1)}, bf16[256,128]{1,0:T(8,128)(2,1)}, u32[]{:S(2)}) copy-start(bf16[256,128]{1,0:T(8,128)(2,1)} %get-tuple-element.21) | copy-start | bytes 196612
  62.4 2.2 %copy-start = (f32[256,128]{1,0:T(8,128)S(1)}, f32[256,128]{1,0:T(8,128)}, u32[]{:S(2)}) copy-start(f32[256,128]{1,0:T(8,128)} %get-tuple-element.22) | copy-start | bytes 393220
  64.6 0.9 %copy-start.1 = (f32[64,256]{1,0:T(8,128)S(1)}, f32[64,256]{1,0:T(8,128)}, u32[]{:S(2)}) copy-start(f32[64,256]{1,0:T(8,128)} %get-tuple-element.23) | copy-start | bytes 196612
  65.4 0.6 copy-start.3

commit v2 on v1

v2 whole, which is shorter than its diff:
```python
import jax
import jax.numpy as jnp
from jax import lax
from jax.experimental import pallas as pl
from jax.experimental.pallas import tpu as pltpu
from jax.sharding import PartitionSpec as P

DK = 128
DV = 256
T = 256
BLK = 32
NB = T // BLK
NZ, NX, NT = 8, 4, 8
SLAB = DV // NX
ROWS = 64
MESH = pl.DeviceIdType.MESH
F32, BF16 = jnp.float32, jnp.bfloat16


def dot(a, b):
    return jnp.dot(a, b, preferred_element_type=F32)


def dot_nt(a, b):
    return lax.dot_general(a, b, (((1,), (1,)), ((), ())), preferred_element_type=F32)


def dot_tn(a, b):
    return lax.dot_general(a, b, (((0,), (0,)), ((), ())), preferred_element_type=F32)


def exact_sum(ones, a):
    hi = a.astype(BF16)
    rest = a - hi.astype(F32)
    mid = rest.astype(BF16)
    low = (rest - mid.astype(F32)).astype(BF16)
    return dot(ones, hi) + (dot(ones, mid) + dot(ones, low))


def kernel(
    x_hbm, q_hbm, k_hbm, w_hbm, g_hbm, do_hbm,
    dq_hbm, dk_hbm, dg_hbm, dw_hbm, rn_hbm,
    x_v, q_v, k_v, w_v, g_v, do_v, dq_v, dk_v, dg_v, dwo_v, rn_v,
    xt_v, val_v, locs_v, adjs_v, as_v, vgs_v, xb_v,
    x1s, x1r, z2s, z2r, x3s, x3r, gx, xts, xg, dwp, rzr, tps, tpr,
    in_sem, out_sem, x1_ss, x1_rs, z2_ss, z2_rs, x3_ss, x3_rs, gx_ss, gx_rs, xx_ss, xx_rs, xy_ss, xy_rs,
    xc_ss, xc_rs, rz_ss, rz_rs, tp_ss, tp_rs,
):
    sp, tp = lax.axis_index("sp"), lax.axis_index("tp")
    z, x = sp // NX, lax.rem(sp, NX)

    def x_dev(t):
        return {"sp": z * NX + t}

    def z_dev(t):
        return {"sp": t * NX + x}

    def tp_dev(t):
        return {"tp": t}

    barrier = pltpu.get_barrier_semaphore()
    for k in range(1, NX):
        pl.semaphore_signal(barrier, inc=1, device_id=x_dev(lax.rem(x + k, NX)), device_id_type=MESH)
    for k in range(1, NZ):
        pl.semaphore_signal(barrier, inc=1, device_id=z_dev(lax.rem(z + k, NZ)), device_id_type=MESH)
    for k in range(1, NT):
        pl.semaphore_signal(barrier, inc=1, device_id=tp_dev(lax.rem(tp + k, NT)), device_id_type=MESH)

    loads = [
        pltpu.make_async_copy(src, dst, in_sem.at[i])
        for i, (src, dst) in enumerate(
            ((g_hbm, g_v), (q_hbm, q_v), (do_hbm, do_v), (k_hbm, k_v), (x_hbm, x_v), (w_hbm, w_v))
        )
    ]
    for load in loads:
        load.start()

    started = []

    def go(cp):
        cp.start()
        started.append(cp)

    def remote(src, dst, ss, rs, dev):
        return pltpu.make_async_remote_copy(
            src_ref=src, dst_ref=dst, send_sem=ss, recv_sem=rs, device_id=dev, device_id_type=MESH
        )

    row = lax.broadcasted_iota(jnp.int32, (T, T), 0)
    col = lax.broadcasted_iota(jnp.int32, (T, T), 1)
    same = (row >> 5) == (col >> 5)
    lower = same & (col <= row)
    upper = same & (col >= row)

    loads[0].wait()
    c = exact_sum(lower.astype(BF16), g_v[...])
    c3 = c.reshape(NB, BLK, DK)
    ends = [c3[b, BLK - 1 : BLK, :] for b in range(NB)]
    before = [jnp.zeros((1, DK), F32)]
    for b in range(NB):
        before.append(before[-1] + ends[b])
    after = [jnp.zeros((1, DK), F32)]
    for b in reversed(range(1, NB)):
        after.append(after[-1] + ends[b])
    after = after[::-1]
    total = before[NB]

    def per_block(rows):
        return jnp.concatenate([jnp.broadcast_to(r, (BLK, DK)) for r in rows], axis=0)

    end_wide = per_block(ends)
    from_start = jnp.exp(c + per_block(before[:NB]))
    tail_log = end_wide - c
    to_end = jnp.exp(tail_log + per_block(after))
    span_decay = jnp.exp(total)

    loads[1].wait()
    loads[2].wait()
    qs = q_v[...].astype(F32) * (DK**-0.5)
    do = do_v[...]
    span_adj = dot_tn(do, (qs * from_start).astype(BF16))
    wide_decay = jnp.broadcast_to(span_decay, (8, DK))
    for s in range(NX):
        x1s[0, s, :SLAB, :] = span_adj[s * SLAB : (s + 1) * SLAB]
        x1s[0, s, SLAB:, :] = wide_decay

    loads[3].wait()
    kf = k_v[...].astype(F32)
    exp_c = jnp.exp(c)
    exp_nc = jnp.exp(-c)
    exp_tail = jnp.exp(tail_log)
    grown_q = (qs * exp_c).astype(BF16)
    shrunk_k = (kf * exp_nc).astype(BF16)
    tail_k = (kf * exp_tail).astype(BF16)
    k_end = kf * to_end
    adj = jnp.zeros((DV, DK), F32)
    for b in reversed(range(NB)):
        sl = slice(b * BLK, (b + 1) * BLK)
        adjs_v[b] = adj.astype(BF16)
        if b:
            adj = jnp.exp(ends[b]) * adj + dot_tn(do[sl], grown_q[sl])
    key_dots_t = jnp.where(upper, dot_nt(shrunk_k, grown_q), 0.0).astype(BF16)
    local_vg = dot(key_dots_t, do) + jnp.concatenate(
        [dot_nt(tail_k[b * BLK : (b + 1) * BLK], adjs_v[b]) for b in range(NB)], axis=0
    )
    gx[x, 0] = local_vg[:, :DK]
    gx[x, 1] = local_vg[:, DK:]
    gx[x, 2] = k_end
    gx[x, 3] = span_adj

    loads[4].wait()
    for zz in range(NZ):
        xt_v[:, zz] = x_v[:, zz * NX * ROWS : (zz + 1) * NX * ROWS].T.reshape(NX, ROWS, T)
    for t in range(NX):
        xts[t] = xt_v[t, tp].astype(F32)
    pl.semaphore_wait(barrier, NX - 1 + NZ - 1 + NT - 1)

    def x1_copy(i, k, src, slot, to):
        return remote(x1s.at[i, src], x1r.at[i, slot], x1_ss.at[i, k], x1_rs.at[i, k], x_dev(to))

    def x_leg(i):
        for k in (2, 1, 3):
            t = lax.rem(x + k, NX)
            go(x1_copy(i, k, t, x, t))
        x1r[i, x] = x1s[i, x]

    def x_leg_wait(i):
        for k in (2, 1, 3):
            t = lax.rem(x + NX - k, NX)
            x1_copy(i, k, t, t, t).wait_recv()

    x_leg(0)

    def xx_copy(k, t):
        return remote(xts.at[t], xg.at[tp, 3 - k], xx_ss.at[k], xx_rs.at[k], x_dev(t))

    for k in (2, 1, 3):
        go(xx_copy(k, lax.rem(x + k, NX)))

    right, left, far = lax.rem(x + 1, NX), lax.rem(x + 3, NX), lax.rem(x + 2, NX)

    def gx_copy(n, slot, part, to):
        ref = gx.at[slot, pl.ds(part, 2)]
        return remote(ref, ref, gx_ss.at[n], gx_rs.at[n], x_dev(to))

    go(gx_copy(0, x, 0, right))
    go(gx_copy(1, x, 2, left))
    go(gx_copy(2, x, 2, right))
    go(gx_copy(3, x, 0, left))

    loads[5].wait()
    val_v[...] = dot(x_v[...], w_v[...]).astype(BF16)
    v = val_v[...]
    span_state = dot_tn(v, k_end.astype(BF16))
    for s in range(NX):
        x1s[1, s, :SLAB, :] = span_state[s * SLAB : (s + 1) * SLAB]
        x1s[1, s, SLAB:, :] = wide_decay
    x_leg(1)

    def slab(i, t):
        return x1r[i, t, :SLAB, :]

    def slab_decay(i, t):
        return x1r[i, t, SLAB : SLAB + 1, :]

    def group_total(i, order):
        x_leg_wait(i)
        acc = slab(i, order[0])
        dec = slab_decay(i, order[0])
        for t in order[1:]:
            acc = slab(i, t) + slab_decay(i, t) * acc
            dec = dec * slab_decay(i, t)
        z2s[i, :SLAB, :] = acc
        z2s[i, SLAB:, :] = jnp.broadcast_to(dec, (8, DK))

    def z_copy(i, k, t, slot):
        return remote(z2s.at[i], z2r.at[i, slot], z2_ss.at[i, k], z2_rs.at[i, k], z_dev(t))

    group_total(0, (3, 2, 1, 0))
    for k in (4, 3, 5, 2, 6, 1, 7):
        @pl.when(z >= k)
        def _():
            z_copy(0, k, z - k, z).start()

    sibling = tp + 1 - 2 * lax.rem(tp, 2)

    def xy_copy(j, slot, to):
        return remote(xg.at[slot], xg.at[slot], xy_ss.at[j], xy_rs.at[j], tp_dev(to))

    def xc_copy(j, slot):
        return remote(xg.at[slot], xg.at[slot], xc_ss.at[j], xc_rs.at[j], tp_dev(sibling))

    for k in (1, 3, 2):
        xx_copy(k, lax.rem(x + NX - k, NX)).wait_recv()
    for j in (2, 1, 3):
        go(xy_copy(j, tp, lax.rem(tp + 2 * j, NT)))
    go(xc_copy(0, tp))

    gx_copy(0, left, 0, right).wait_recv()
    go(gx_copy(4, left, 0, right))
    gx_copy(1, right, 2, left).wait_recv()
    go(gx_copy(5, right, 2, left))

    def adj_step(n, acc):
        t = NZ - 1 - n
        z_copy(0, t - z, t, t).wait_recv()
        return z2r[0, t, :SLAB, :] + z2r[0, t, SLAB : SLAB + 1, :] * acc

    x3s[0, 0] = lax.fori_loop(0, NZ - 1 - z, adj_step, jnp.zeros((SLAB, DK), F32))

    def x3_copy(i, k, src, slot, to):
        return remote(x3s.at[i, src], x3r.at[i, slot], x3_ss.at[i, k], x3_rs.at[i, k], x_dev(to))

    def x3_wait(i):
        for k in (2, 1, 3):
            t = lax.rem(x + NX - k, NX)
            x3_copy(i, k, 0, t, t).wait_recv()

    for k in (2, 1, 3):
        go(x3_copy(0, k, 0, x, lax.rem(x + k, NX)))
    x3r[0, x] = x3s[0, 0]

    group_total(1, (0, 1, 2, 3))
    for k in (4, 3, 5, 2, 6, 1, 7):
        @pl.when(z + k < NZ)
        def _():
            z_copy(1, k, z + k, z).start()

    for j in (1, 3, 2):
        slot = lax.rem(tp + NT - 2 * j, NT)
        xy_copy(j, slot, slot).wait_recv()
        go(xc_copy(j, slot))
    for j in (0, 1, 3, 2):
        xc_copy(j, lax.rem(sibling + NT - 2 * j, NT)).wait_recv()

    def columns(t):
        return pl.ds(pl.multiple_of(t * T, T), T)

    xb_v[:, :, columns(x)] = xt_v[x]
    for k in range(1, NX):
        xb_v[:, :, columns(lax.rem(x + k, NX))] = xg[:, k - 1].astype(BF16)

    gx_copy(2, left, 2, left).wait_recv()
    gx_copy(3, right, 0, right).wait_recv()
    gx_copy(4, far, 0, left).wait_recv()
    gx_copy(5, far, 2, right).wait_recv()
    x3_wait(0)

    acc = x3r[0].reshape(DV, DK)
    for t in (3, 2, 1, 0):
        as_v[t] = acc
        k_t = gx[t, 2].astype(BF16)
        acc16 = acc.astype(BF16)
        for h in range(2):
            hl = slice(h * DK, (h + 1) * DK)
            vgs_v[t * T : (t + 1) * T, hl] = (gx[t, h] + dot_nt(k_t, acc16[hl])).astype(BF16)
        if t:
            acc = gx[t, 3] + slab_decay(0, t) * acc
    dwp[...] = dot(xb_v[...].reshape(NZ * ROWS, NX * T), vgs_v[...]).reshape(NZ, ROWS, DV)

    def rz_copy(k, src, slot, to):
        return remote(dwp.at[src], rzr.at[slot], rz_ss.at[k], rz_rs.at[k], z_dev(to))

    for k in (4, 3, 5, 2, 6, 1, 7):
        t = lax.rem(z + k, NZ)
        go(rz_copy(k, t, z, t))
    adj_in = as_v[x]
    adj_in16 = adj_in.astype(BF16)

    state = jnp.zeros((DV, DK), F32)
    for b in range(NB):
        sl = slice(b * BLK, (b + 1) * BLK)
        locs_v[b] = state.astype(BF16)
        if b < NB - 1:
            state = jnp.exp(ends[b]) * state + dot_tn(v[sl], tail_k[sl])
    out_dots = jnp.where(lower, dot_nt(do, v), 0.0).astype(BF16)
    out_dots_t = jnp.where(upper, dot_nt(v, do), 0.0).astype(BF16)
    local_qg = dot(out_dots, shrunk_k) + jnp.concatenate(
        [dot(do[b * BLK : (b + 1) * BLK], locs_v[b]) for b in range(NB)], axis=0
    )
    local_kg = exp_nc * dot(out_dots_t, grown_q) + exp_tail * jnp.concatenate(
        [dot(v[b * BLK : (b + 1) * BLK], adjs_v[b]) for b in range(NB)], axis=0
    )
    kg = local_kg + to_end * dot(v, adj_in16)
    dk_v[...] = kg.astype(BF16)

    def state_step(t, acc):
        z_copy(1, z - t, t, t).wait_recv()
        return z2r[1, t, :SLAB, :] + z2r[1, t, SLAB : SLAB + 1, :] * acc

    acc = lax.fori_loop(0, z, state_step, jnp.zeros((SLAB, DK), F32))
    for t in range(NX):
        x3s[1, t] = acc
        if t < NX - 1:
            acc = slab(1, t) + slab_decay(1, t) * acc
    for k in (2, 1, 3):
        t = lax.rem(x + k, NX)
        go(x3_copy(1, k, t, x, t))
    x3r[1, x] = x3s[1, x]
    x3_wait(1)
    state_in = x3r[1].reshape(DV, DK)
    qg = exp_c * local_qg + from_start * dot(do, state_in.astype(BF16))
    dq_v[...] = (qg * (DK**-0.5)).astype(BF16)
    carry = jnp.sum(adj_in * (span_state + span_decay * state_in), axis=0, keepdims=True)
    dg_v[...] = exact_sum((col >= row).astype(BF16), qs * qg - kf * kg) + carry
    stores = [
        pltpu.make_async_copy(src, dst, out_sem.at[i])
        for i, (src, dst) in enumerate(((dq_v, dq_hbm), (dk_v, dk_hbm), (dg_v, dg_hbm), (dwo_v, dw_hbm), (rn_v, rn_hbm)))
    ]
    for store in stores[:3]:
        store.start()

    total_dw = dwp[z]
    for k in (1, 7, 2, 6, 3, 5, 4):
        t = lax.rem(z + NZ - k, NZ)
        rz_copy(k, t, t, t).wait_recv()
        total_dw = total_dw + rzr[t]
    dwo_v[...] = total_dw
    stores[3].start()

    squares = total_dw[:, :DK] * total_dw[:, :DK] + total_dw[:, DK:] * total_dw[:, DK:]
    norms = jnp.sum(squares.T, axis=0, keepdims=True)
    tps[...] = jnp.broadcast_to(jnp.concatenate([norms, jnp.zeros((1, 64), F32)], axis=1), (8, 128))

    def tp_copy(k, slot, to):
        return remote(tps, tpr.at[slot], tp_ss.at[k], tp_rs.at[k], tp_dev(to))

    for k in range(1, NT):
        go(tp_copy(k, tp, lax.rem(tp + k, NT)))
    acc = tps[0:1, :]
    for k in range(1, NT):
        t = lax.rem(tp + NT - k, NT)
        tp_copy(k, t, t).wait_recv()
        acc = acc + tpr[t, 0:1, :]
    rn_v[...] = acc[:, :ROWS]
    stores[4].start()

    for cp in started:
        cp.wait_send()
    for k in range(1, NZ):
        @pl.when(z >= k)
        def _():
            z_copy(0, k, z - k, z).wait_send()

        @pl.when(z + k < NZ)
        def _():
            z_copy(1, k, z + k, z).wait_send()
    for store in stores:
        store.wait()


def on_device(block_input, queries, keys, w_value, log_decay, d_out):
    any_spec = pl.BlockSpec(memory_space=pl.ANY)
    dma, vmem = pltpu.SemaphoreType.DMA, pltpu.VMEM
    outs = pl.pallas_call(
        kernel,
        out_shape=(
            jax.ShapeDtypeStruct((T, DK), BF16),
            jax.ShapeDtypeStruct((T, DK), BF16),
            jax.ShapeDtypeStruct((T, DK), F32),
            jax.ShapeDtypeStruct((ROWS, DV), F32),
            jax.ShapeDtypeStruct((1, ROWS), F32),
        ),
        in_specs=[any_spec] * 6,
        out_specs=(any_spec,) * 5,
        scratch_shapes=[
            vmem((T, 2048), BF16), vmem((T, DK), BF16), vmem((T, DK), BF16),
            vmem((2048, DV), BF16), vmem((T, DK), F32), vmem((T, DV), BF16),
            vmem((T, DK), BF16), vmem((T, DK), BF16), vmem((T, DK), F32),
            vmem((ROWS, DV), F32), vmem((1, ROWS), F32),
            vmem((NX, NZ, ROWS, T), BF16), vmem((T, DV), BF16),
            vmem((NB, DV, DK), BF16), vmem((NB, DV, DK), BF16),
            vmem((NX, DV, DK), F32), vmem((NX * T, DV), BF16), vmem((NZ, ROWS, NX * T), BF16),
            vmem((2, NX, SLAB + 8, DK), F32), vmem((2, NX, SLAB + 8, DK), F32),
            vmem((2, SLAB + 8, DK), F32), vmem((2, NZ, SLAB + 8, DK), F32),
            vmem((2, NX, SLAB, DK), F32), vmem((2, NX, SLAB, DK), F32),
            vmem((NX, 4, T, DK), F32), vmem((NX, ROWS, T), F32), vmem((NT, NX - 1, ROWS, T), F32),
            vmem((NZ, ROWS, DV), F32), vmem((NZ, ROWS, DV), F32),
            vmem((8, 128), F32), vmem((NT, 8, 128), F32),
            dma((6,)), dma((5,)), dma((2, NX)), dma((2, NX)), dma((2, NZ)), dma((2, NZ)),
            dma((2, NX)), dma((2, NX)), dma((6,)), dma((6,)), dma((NX,)), dma((NX,)), dma((NX,)), dma((NX,)),
            dma((NX,)), dma((NX,)), dma((NZ,)), dma((NZ,)), dma((NT,)), dma((NT,)),
        ],
        compiler_params=pltpu.CompilerParams(collective_id=0, has_side_effects=True),
        name="gla_backward",
    )(block_input, queries, keys, w_value, log_decay, d_out)
    return (*outs[:4], outs[4].reshape(ROWS))


def solution(mesh):
    in_specs = (P("sp", None), P("sp", "tp"), P("sp", "tp"), P(None, "tp"), P("sp", "tp"), P("sp", "tp"))
    out_specs = (P("sp", "tp"), P("sp", "tp"), P("sp", "tp"), P("sp", "tp"), P("sp"))
    return jax.shard_map(on_device, mesh=mesh, in_specs=in_specs, out_specs=out_specs, check_vma=False)
```

time: 66.7 us -> 61.8 us (0.927)
  Pallas kernels: 61.7 us -> 56.8 us
    pallas_call x1, Pallas kernels: 61.7 us -> 56.8 us  [on_device(): pl.pallas_call(kernel, out_shape=(jax.ShapeDtypeStruct((T, DK), BF16), ja...]
where the time goes in v2:
time: 61.8 us; the launch traced here: 61.6 us
  Pallas kernels  56.8 us (92%)
  local copies, waits for them, and re-layouts  4.16 us (7%)
  between operations  0.66 us (1%)
    pallas_call x1, Pallas kernels, on_device(): pl.pallas_call(kernel, out_shape=(jax.ShapeDtypeStruct((T, DK), BF16), ja...  56.8 us
    unnamed x13, local copies, waits for them, and re-layouts  4.16 us

profile of v2, /device:TPU:1, one launch (start us, length us, event | category | flops | bytes accessed | tf_op | source)
XLA Modules:
  0.0 61.6 jit_solution(6936723929798114971)
XLA Ops:
  0.6 56.8 %gla_backward.1 = (bf16[256,128]{1,0:T(8,128)(2,1)}, bf16[256,128]{1,0:T(8,128)(2,1)}, f32[256,128]{1,0:T(8,128)}, f32[64,256]{1,0:T(8,128)}, f32[1,64]{1,0:T(1,128)}) custom-call(bf16[256,2048]{1,0:T(8,128)(2,1)} %x_hbm.1, bf16[256,128]{1,0:T(8,128)(2,1)} %q_hbm.1, bf16[256,128]{1,0:T(8,128)(2,1)} %k_hbm.1, bf16[2048,256]{1,0:T(8,128)(2,1)} %w_hbm.1, ...), custom_call_target="tpu_custom_call" | custom-call | tf_op jit(solution)/shard_map/gla_backward/pallas_call | solution.py:395
  57.4 0.0 copy-start.2
  57.4 0.0 copy-start
  57.4 1.5 %copy.16 = bf16[256,128]{1,0:T(8,128)(2,1)} copy(bf16[256,128]{1,0:T(8,128)(2,1)} %get-tuple-element.20) | data formatting | bytes 131072
  59.0 0.0 copy-done.2
  59.0 0.6 %copy.17 = bf16[256,128]{1,0:T(8,128)(2,1)} copy(bf16[256,128]{1,0:T(8,128)(2,1)S(1)} %copy-done.2) | data formatting | bytes 131072
  59.6 0.0 copy-done
  59.6 0.0 copy-start.1
  59.6 0.7 %copy.18 = f32[256,128]{1,0:T(8,128)} copy(f32[256,128]{1,0:T(8,128)S(1)} %copy-done) | data formatting | bytes 262144
  60.3 0.2 copy-done.1
  60.5 0.0 copy-start.3
  60.5 0.6 %copy.19 = f32[64,256]{1,0:T(8,128)} copy(f32[64,256]{1,0:T(8,128)S(1)} %copy-done.1) | data formatting | bytes 131072
  61.1 0.0 copy-done.3
  61.1 0.5 copy.20
Async XLA Ops:
  57.4 1.5 %copy-start.2 = (bf16[256,128]{1,0:T(8,128)(2,1)S(1)}, bf16[256,128]{1,0:T(8,128)(2,1)}, u32[]{:S(2)}) copy-start(bf16[256,128]{1,0:T(8,128)(2,1)} %get-tuple-element.21) | copy-start | bytes 196612
  57.4 2.2 %copy-start = (f32[256,128]{1,0:T(8,128)S(1)}, f32[256,128]{1,0:T(8,128)}, u32[]{:S(2)}) copy-start(f32[256,128]{1,0:T(8,128)} %get-tuple-element.22) | copy-start | bytes 393220
  59.6 0.9 %copy-start.1 = (f32[64,256]{1,0:T(8,128)S(1)}, f32[64,256]{1,0:T(8,128)}, u32[]{:S(2)}) copy-start(f32[64,256]{1,0:T(8,128)} %get-tuple-element.23) | copy-start | bytes 196612
  60.5 0.6 %copy-start.3 = (f32[1,64]{1,0:T(1,128)S(1)}, f32[1,64]{1,0:T(1,128)}, u32[]{:S(2)}) copy-start(f32[1,64]{1,0:T(1,128)} %get-tuple-element.14) | copy-start | bytes 772

commit v3 on v2

--- a/solution.py
+++ b/solution.py
@@ -39,11 +39,11 @@
 
 def kernel(
     x_hbm, q_hbm, k_hbm, w_hbm, g_hbm, do_hbm,
-    dq_hbm, dk_hbm, dg_hbm, dw_hbm, rn_hbm,
-    x_v, q_v, k_v, w_v, g_v, do_v, dq_v, dk_v, dg_v, dwo_v, rn_v,
+    dq_v, dk_v, dg_v, dwo_v, rn_v,
+    x_v, q_v, k_v, w_v, g_v, do_v,
     xt_v, val_v, locs_v, adjs_v, as_v, vgs_v, xb_v,
-    x1s, x1r, z2s, z2r, x3s, x3r, gx, xts, xg, dwp, rzr, tps, tpr,
-    in_sem, out_sem, x1_ss, x1_rs, z2_ss, z2_rs, x3_ss, x3_rs, gx_ss, gx_rs, xx_ss, xx_rs, xy_ss, xy_rs,
+    x1s, x1r, z2s, z2r, xis, xir, x3s, x3r, gx, xts, xg, dwp, rzr, tps, tpr,
+    in_sem, x1_ss, x1_rs, z2_ss, z2_rs, xi_ss, xi_rs, x3_ss, x3_rs, gx_ss, gx_rs, xx_ss, xx_rs, xy_ss, xy_rs,
     xc_ss, xc_rs, rz_ss, rz_rs, tp_ss, tp_rs,
 ):
     sp, tp = lax.axis_index("sp"), lax.axis_index("tp")
@@ -143,10 +143,8 @@
     local_vg = dot(key_dots_t, do) + jnp.concatenate(
         [dot_nt(tail_k[b * BLK : (b + 1) * BLK], adjs_v[b]) for b in range(NB)], axis=0
     )
-    gx[x, 0] = local_vg[:, :DK]
-    gx[x, 1] = local_vg[:, DK:]
-    gx[x, 2] = k_end
-    gx[x, 3] = span_adj
+    gx[x, 4] = k_end[: T // 2]
+    gx[x, 5] = k_end[T // 2 :]
 
     loads[4].wait()
     for zz in range(NZ):
@@ -178,15 +176,30 @@
         go(xx_copy(k, lax.rem(x + k, NX)))
 
     right, left, far = lax.rem(x + 1, NX), lax.rem(x + 3, NX), lax.rem(x + 2, NX)
-
-    def gx_copy(n, slot, part, to):
-        ref = gx.at[slot, pl.ds(part, 2)]
-        return remote(ref, ref, gx_ss.at[n], gx_rs.at[n], x_dev(to))
-
-    go(gx_copy(0, x, 0, right))
-    go(gx_copy(1, x, 2, left))
-    go(gx_copy(2, x, 2, right))
-    go(gx_copy(3, x, 0, left))
+    ways = (right, left, right, left)
+
+    def gx_copy(kind, piece, slot):
+        ref = gx.at[slot, piece]
+        return remote(ref, ref, gx_ss.at[kind, piece], gx_rs.at[kind, piece], x_dev(ways[kind]))
+
+    def gx_own(first, second):
+        for a, b in zip(first + second, second + first):
+            go(gx_copy(0, a, x))
+            go(gx_copy(1, b, x))
+
+    def gx_forward(first, second):
+        for a, b in zip(first, second):
+            gx_copy(0, a, left).wait_recv()
+            go(gx_copy(2, a, left))
+            gx_copy(1, b, right).wait_recv()
+            go(gx_copy(3, b, right))
+
+    def gx_wait(first, second):
+        for a, b in zip(first, second):
+            gx_copy(0, b, left).wait_recv()
+            gx_copy(1, a, right).wait_recv()
+            gx_copy(2, a, far).wait_recv()
+            gx_copy(3, b, far).wait_recv()
 
     loads[5].wait()
     val_v[...] = dot(x_v[...], w_v[...]).astype(BF16)
@@ -203,24 +216,32 @@
     def slab_decay(i, t):
         return x1r[i, t, SLAB : SLAB + 1, :]
 
-    def group_total(i, order):
-        x_leg_wait(i)
-        acc = slab(i, order[0])
-        dec = slab_decay(i, order[0])
-        for t in order[1:]:
-            acc = slab(i, t) + slab_decay(i, t) * acc
-            dec = dec * slab_decay(i, t)
-        z2s[i, :SLAB, :] = acc
-        z2s[i, SLAB:, :] = jnp.broadcast_to(dec, (8, DK))
-
     def z_copy(i, k, t, slot):
         return remote(z2s.at[i], z2r.at[i, slot], z2_ss.at[i, k], z2_rs.at[i, k], z_dev(t))
 
-    group_total(0, (3, 2, 1, 0))
+    x_leg_wait(0)
+    inner = [None] * NX
+    inner[3] = jnp.zeros((SLAB, DK), F32)
+    for t in (2, 1, 0):
+        inner[t] = slab(0, t + 1) + slab_decay(0, t + 1) * inner[t + 1]
+    row_decay = slab_decay(0, 0) * slab_decay(0, 1) * slab_decay(0, 2) * slab_decay(0, 3)
+    z2s[0, :SLAB, :] = slab(0, 0) + slab_decay(0, 0) * inner[0]
+    z2s[0, SLAB:, :] = jnp.broadcast_to(row_decay, (8, DK))
     for k in (4, 3, 5, 2, 6, 1, 7):
         @pl.when(z >= k)
         def _():
             z_copy(0, k, z - k, z).start()
+
+    def xi_copy(k, src, slot, to):
+        return remote(xis.at[src], xir.at[slot], xi_ss.at[k], xi_rs.at[k], x_dev(to))
+
+    for t in range(NX):
+        xis[t] = inner[t]
+    for k in (2, 1, 3):
+        t = lax.rem(x + k, NX)
+        go(xi_copy(k, t, x, t))
+    xir[x] = xis[x]
+    gx_own((4,), (5,))
 
     sibling = tp + 1 - 2 * lax.rem(tp, 2)
 
@@ -236,10 +257,16 @@
         go(xy_copy(j, tp, lax.rem(tp + 2 * j, NT)))
     go(xc_copy(0, tp))
 
-    gx_copy(0, left, 0, right).wait_recv()
-    go(gx_copy(4, left, 0, right))
-    gx_copy(1, right, 2, left).wait_recv()
-    go(gx_copy(5, right, 2, left))
+    for k in (2, 1, 3):
+        t = lax.rem(x + NX - k, NX)
+        xi_copy(k, t, t, t).wait_recv()
+    adj_row = xir[...].reshape(DV, DK)
+    row_vg = local_vg + dot_nt(k_end.astype(BF16), adj_row.astype(BF16))
+    for h in range(2):
+        for p in range(2):
+            gx[x, 2 * h + p] = row_vg[p * 128 : (p + 1) * 128, h * DK : (h + 1) * DK]
+    gx_own((0, 1), (2, 3))
+    gx_forward((4,), (5,))
 
     def adj_step(n, acc):
         t = NZ - 1 - n
@@ -260,7 +287,13 @@
         go(x3_copy(0, k, 0, x, lax.rem(x + k, NX)))
     x3r[0, x] = x3s[0, 0]
 
-    group_total(1, (0, 1, 2, 3))
+    gx_forward((0, 1), (2, 3))
+    x_leg_wait(1)
+    acc = slab(1, 0)
+    for t in range(1, NX):
+        acc = slab(1, t) + slab_decay(1, t) * acc
+    z2s[1, :SLAB, :] = acc
+    z2s[1, SLAB:, :] = jnp.broadcast_to(row_decay, (8, DK))
     for k in (4, 3, 5, 2, 6, 1, 7):
         @pl.when(z + k < NZ)
         def _():
@@ -280,31 +313,31 @@
     for k in range(1, NX):
         xb_v[:, :, columns(lax.rem(x + k, NX))] = xg[:, k - 1].astype(BF16)
 
-    gx_copy(2, left, 2, left).wait_recv()
-    gx_copy(3, right, 0, right).wait_recv()
-    gx_copy(4, far, 0, left).wait_recv()
-    gx_copy(5, far, 2, right).wait_recv()
+    gx_wait((4,), (5,))
+    gx_wait((0, 1), (2, 3))
     x3_wait(0)
 
     acc = x3r[0].reshape(DV, DK)
     for t in (3, 2, 1, 0):
         as_v[t] = acc
-        k_t = gx[t, 2].astype(BF16)
+        k_t = gx[t, 4:6].reshape(T, DK).astype(BF16)
         acc16 = acc.astype(BF16)
         for h in range(2):
             hl = slice(h * DK, (h + 1) * DK)
-            vgs_v[t * T : (t + 1) * T, hl] = (gx[t, h] + dot_nt(k_t, acc16[hl])).astype(BF16)
+            vgs_v[t * T : (t + 1) * T, hl] = (gx[t, 2 * h : 2 * h + 2].reshape(T, DK) + dot_nt(k_t, acc16[hl])).astype(BF16)
         if t:
-            acc = gx[t, 3] + slab_decay(0, t) * acc
+            acc = slab_decay(0, t) * acc
     dwp[...] = dot(xb_v[...].reshape(NZ * ROWS, NX * T), vgs_v[...]).reshape(NZ, ROWS, DV)
 
     def rz_copy(k, src, slot, to):
         return remote(dwp.at[src], rzr.at[slot], rz_ss.at[k], rz_rs.at[k], z_dev(to))
 
+    late = []
     for k in (4, 3, 5, 2, 6, 1, 7):
         t = lax.rem(z + k, NZ)
-        go(rz_copy(k, t, z, t))
-    adj_in = as_v[x]
+        late.append(rz_copy(k, t, z, t))
+        late[-1].start()
+    adj_in = adj_row + as_v[x]
     adj_in16 = adj_in.astype(BF16)
 
     state = jnp.zeros((DV, DK), F32)
@@ -343,12 +376,16 @@
     dq_v[...] = (qg * (DK**-0.5)).astype(BF16)
     carry = jnp.sum(adj_in * (span_state + span_decay * state_in), axis=0, keepdims=True)
     dg_v[...] = exact_sum((col >= row).astype(BF16), qs * qg - kf * kg) + carry
-    stores = [
-        pltpu.make_async_copy(src, dst, out_sem.at[i])
-        for i, (src, dst) in enumerate(((dq_v, dq_hbm), (dk_v, dk_hbm), (dg_v, dg_hbm), (dwo_v, dw_hbm), (rn_v, rn_hbm)))
-    ]
-    for store in stores[:3]:
-        store.start()
+    for cp in started:
+        cp.wait_send()
+    for k in range(1, NZ):
+        @pl.when(z >= k)
+        def _():
+            z_copy(0, k, z - k, z).wait_send()
+
+        @pl.when(z + k < NZ)
+        def _():
+            z_copy(1, k, z + k, z).wait_send()
 
     total_dw = dwp[z]
     for k in (1, 7, 2, 6, 3, 5, 4):
@@ -356,7 +393,6 @@
         rz_copy(k, t, t, t).wait_recv()
         total_dw = total_dw + rzr[t]
     dwo_v[...] = total_dw
-    stores[3].start()
 
     squares = total_dw[:, :DK] * total_dw[:, :DK] + total_dw[:, DK:] * total_dw[:, DK:]
     norms = jnp.sum(squares.T, axis=0, keepdims=True)
@@ -366,64 +402,69 @@
         return remote(tps, tpr.at[slot], tp_ss.at[k], tp_rs.at[k], tp_dev(to))
 
     for k in range(1, NT):
-        go(tp_copy(k, tp, lax.rem(tp + k, NT)))
+        late.append(tp_copy(k, tp, lax.rem(tp + k, NT)))
+        late[-1].start()
     acc = tps[0:1, :]
     for k in range(1, NT):
         t = lax.rem(tp + NT - k, NT)
         tp_copy(k, t, t).wait_recv()
         acc = acc + tpr[t, 0:1, :]
     rn_v[...] = acc[:, :ROWS]
-    stores[4].start()
-
-    for cp in started:
+    for cp in late:
         cp.wait_send()
-    for k in range(1, NZ):
-        @pl.when(z >= k)
-        def _():
-            z_copy(0, k, z - k, z).wait_send()
-
-        @pl.when(z + k < NZ)
-        def _():
-            z_copy(1, k, z + k, z).wait_send()
-    for store in stores:
-        store.wait()
+
+
+def finish(*refs):
+    ins, outs, sem = refs[:5], refs[5:10], refs[10]
+    copies = [pltpu.make_async_copy(src, dst, sem.at[i]) for i, (src, dst) in enumerate(zip(ins, outs))]
+    for cp in copies:
+        cp.start()
+    for cp in copies:
+        cp.wait()
 
 
 def on_device(block_input, queries, keys, w_value, log_decay, d_out):
-    any_spec = pl.BlockSpec(memory_space=pl.ANY)
     dma, vmem = pltpu.SemaphoreType.DMA, pltpu.VMEM
+    hbm_spec, vmem_spec = pl.BlockSpec(memory_space=pltpu.HBM), pl.BlockSpec(memory_space=vmem)
+    shapes = (((T, DK), BF16), ((T, DK), BF16), ((T, DK), F32), ((ROWS, DV), F32), ((1, ROWS), F32))
+    args = [
+        pltpu.with_memory_space_constraint(a, pltpu.HBM)
+        for a in (block_input, queries, keys, w_value, log_decay, d_out)
+    ]
     outs = pl.pallas_call(
         kernel,
-        out_shape=(
-            jax.ShapeDtypeStruct((T, DK), BF16),
-            jax.ShapeDtypeStruct((T, DK), BF16),
-            jax.ShapeDtypeStruct((T, DK), F32),
-            jax.ShapeDtypeStruct((ROWS, DV), F32),
-            jax.ShapeDtypeStruct((1, ROWS), F32),
-        ),
-        in_specs=[any_spec] * 6,
-        out_specs=(any_spec,) * 5,
+        out_shape=tuple(vmem(*s) for s in shapes),
+        in_specs=[hbm_spec] * 6,
+        out_specs=(vmem_spec,) * 5,
         scratch_shapes=[
             vmem((T, 2048), BF16), vmem((T, DK), BF16), vmem((T, DK), BF16),
             vmem((2048, DV), BF16), vmem((T, DK), F32), vmem((T, DV), BF16),
-            vmem((T, DK), BF16), vmem((T, DK), BF16), vmem((T, DK), F32),
-            vmem((ROWS, DV), F32), vmem((1, ROWS), F32),
             vmem((NX, NZ, ROWS, T), BF16), vmem((T, DV), BF16),
             vmem((NB, DV, DK), BF16), vmem((NB, DV, DK), BF16),
             vmem((NX, DV, DK), F32), vmem((NX * T, DV), BF16), vmem((NZ, ROWS, NX * T), BF16),
             vmem((2, NX, SLAB + 8, DK), F32), vmem((2, NX, SLAB + 8, DK), F32),
             vmem((2, SLAB + 8, DK), F32), vmem((2, NZ, SLAB + 8, DK), F32),
+            vmem((NX, SLAB, DK), F32), vmem((NX, SLAB, DK), F32),
             vmem((2, NX, SLAB, DK), F32), vmem((2, NX, SLAB, DK), F32),
-            vmem((NX, 4, T, DK), F32), vmem((NX, ROWS, T), F32), vmem((NT, NX - 1, ROWS, T), F32),
+            vmem((NX, 6, T // 2, DK), F32), vmem((NX, ROWS, T), F32), vmem((NT, NX - 1, ROWS, T), F32),
             vmem((NZ, ROWS, DV), F32), vmem((NZ, ROWS, DV), F32),
             vmem((8, 128), F32), vmem((NT, 8, 128), F32),
-            dma((6,)), dma((5,)), dma((2, NX)), dma((2, NX)), dma((2, NZ)), dma((2, NZ)),
-            dma((2, NX)), dma((2, NX)), dma((6,)), dma((6,)), dma((NX,)), dma((NX,)), dma((NX,)), dma((NX,)),
+            dma((6,)), dma((2, NX)), dma((2, NX)), dma((2, NZ)), dma((2, NZ)), dma((NX,)), dma((NX,)),
+            dma((2, NX)), dma((2, NX)), dma((4, 6)), dma((4, 6)), dma((NX,)), dma((NX,)), dma((NX,)), dma((NX,)),
             dma((NX,)), dma((NX,)), dma((NZ,)), dma((NZ,)), dma((NT,)), dma((NT,)),
         ],
-        compiler_params=pltpu.CompilerParams(collective_id=0, has_side_effects=True),
+        compiler_params=pltpu.CompilerParams(collective_id=0, has_side_effects=True, vmem_limit_bytes=40 << 20),
         name="gla_backward",
-    )(block_input, queries, keys, w_value, log_decay, d_out)
+    )(*args)
+    outs = pl.pallas_call(
+        finish,
+        out_shape=tuple(jax.ShapeDtypeStruct(*s) for s in shapes),
+        in_specs=[pl.BlockSpec(memory_space=pl.ANY)] * 5,
+        out_specs=(hbm_spec,) * 5,
+        scratch_shapes=[dma((5,))],
+        compiler_params=pltpu.CompilerParams(vmem_limit_bytes=1 << 20),
+        name="finish",
+    )(*outs)
     return (*outs[:4], outs[4].reshape(ROWS))
 
 

time: 61.8 us -> 55.4 us (0.90)
  local copies, waits for them, and re-layouts: 4.16 us -> 0 us
  Pallas kernels: 56.8 us -> 54.7 us
    unnamed x13 -> x0, local copies, waits for them, and re-layouts: 4.16 us -> none
    pallas_call x1 -> x2, Pallas kernels: 56.8 us -> 54.7 us  [the longest x1 53.9 us: on_device(): pl.pallas_call(kernel, out_shape=tuple((vmem(*s) for s in shapes)), in_sp...]
where the time goes in v3:
time: 55.4 us; the launch traced here: 55.3 us
  Pallas kernels  54.7 us (99%)
  between operations  0.64 us (1%)
    pallas_call x1, Pallas kernels, on_device(): pl.pallas_call(kernel, out_shape=tuple((vmem(*s) for s in shapes)), in_sp...  53.9 us

profile of v3, /device:TPU:1, one launch (start us, length us, event | category | flops | bytes accessed | tf_op | source)
XLA Modules:
  0.0 55.3 jit_solution(8611384823888888656)
XLA Ops:
  0.6 53.9 %gla_backward.1 = (bf16[256,128]{1,0:T(8,128)(2,1)S(1)}, bf16[256,128]{1,0:T(8,128)(2,1)S(1)}, f32[256,128]{1,0:T(8,128)S(1)}, f32[64,256]{1,0:T(8,128)S(1)}, f32[1,64]{1,0:T(1,128)S(1)}) custom-call(bf16[256,2048]{1,0:T(8,128)(2,1)} %x_hbm.1, bf16[256,128]{1,0:T(8,128)(2,1)} %q_hbm.1, bf16[256,128]{1,0:T(8,128)(2,1)} %k_hbm.1, bf16[2048,256]{1,0:T(8,128)(2,1)} %w_hbm.1, ...), custom_call_target="tpu_custom_call" | custom-call | tf_op jit(solution)/shard_map/gla_backward/pallas_call | solution.py:434
  54.6 0.8 %finish.1 = (bf16[256,128]{1,0:T(8,128)(2,1)}, bf16[256,128]{1,0:T(8,128)(2,1)}, f32[256,128]{1,0:T(8,128)}, f32[64,256]{1,0:T(8,128)}, f32[1,64]{1,0:T(1,128)}) custom-call(bf16[256,128]{1,0:T(8,128)(2,1)S(1)} %get-tuple-element.15.refs_0_, bf16[256,128]{1,0:T(8,128)(2,1)S(1)} %get-tuple-element.16.refs_1_, f32[256,128]{1,0:T(8,128)S(1)} %get-tuple-element.17.refs_2_, ...), custom_call_target="tpu_custom_call" | custom-call | tf_op jit(solution)/shard_map/finish/pallas_call | solution.py:459

commit v4 on v3

--- a/solution.py
+++ b/solution.py
@@ -172,7 +172,7 @@
     def xx_copy(k, t):
         return remote(xts.at[t], xg.at[tp, 3 - k], xx_ss.at[k], xx_rs.at[k], x_dev(t))
 
-    for k in (2, 1, 3):
+    for k in (1, 3, 2):
         go(xx_copy(k, lax.rem(x + k, NX)))
 
     right, left, far = lax.rem(x + 1, NX), lax.rem(x + 3, NX), lax.rem(x + 2, NX)
@@ -245,17 +245,19 @@
 
     sibling = tp + 1 - 2 * lax.rem(tp, 2)
 
-    def xy_copy(j, slot, to):
-        return remote(xg.at[slot], xg.at[slot], xy_ss.at[j], xy_rs.at[j], tp_dev(to))
-
-    def xc_copy(j, slot):
-        return remote(xg.at[slot], xg.at[slot], xc_ss.at[j], xc_rs.at[j], tp_dev(sibling))
+    def xy_copy(j, k, slot, to):
+        ref = xg.at[slot, k]
+        return remote(ref, ref, xy_ss.at[j, k], xy_rs.at[j, k], tp_dev(to))
+
+    def xc_copy(j, k, slot):
+        ref = xg.at[slot, k]
+        return remote(ref, ref, xc_ss.at[j, k], xc_rs.at[j, k], tp_dev(sibling))
 
     for k in (1, 3, 2):
         xx_copy(k, lax.rem(x + NX - k, NX)).wait_recv()
-    for j in (2, 1, 3):
-        go(xy_copy(j, tp, lax.rem(tp + 2 * j, NT)))
-    go(xc_copy(0, tp))
+        for j in (2, 1, 3):
+            go(xy_copy(j, 3 - k, tp, lax.rem(tp + 2 * j, NT)))
+        go(xc_copy(0, 3 - k, tp))
 
     for k in (2, 1, 3):
         t = lax.rem(x + NX - k, NX)
@@ -265,7 +267,7 @@
     for h in range(2):
         for p in range(2):
             gx[x, 2 * h + p] = row_vg[p * 128 : (p + 1) * 128, h * DK : (h + 1) * DK]
-    gx_own((0, 1), (2, 3))
+    gx_own((0,), (1,))
     gx_forward((4,), (5,))
 
     def adj_step(n, acc):
@@ -287,7 +289,8 @@
         go(x3_copy(0, k, 0, x, lax.rem(x + k, NX)))
     x3r[0, x] = x3s[0, 0]
 
-    gx_forward((0, 1), (2, 3))
+    gx_forward((0,), (1,))
+    gx_own((2,), (3,))
     x_leg_wait(1)
     acc = slab(1, 0)
     for t in range(1, NX):
@@ -299,12 +302,14 @@
         def _():
             z_copy(1, k, z + k, z).start()
 
-    for j in (1, 3, 2):
-        slot = lax.rem(tp + NT - 2 * j, NT)
-        xy_copy(j, slot, slot).wait_recv()
-        go(xc_copy(j, slot))
+    for k in (1, 3, 2):
+        for j in (1, 3, 2):
+            slot = lax.rem(tp + NT - 2 * j, NT)
+            xy_copy(j, 3 - k, slot, slot).wait_recv()
+            go(xc_copy(j, 3 - k, slot))
     for j in (0, 1, 3, 2):
-        xc_copy(j, lax.rem(sibling + NT - 2 * j, NT)).wait_recv()
+        for k in (1, 3, 2):
+            xc_copy(j, 3 - k, lax.rem(sibling + NT - 2 * j, NT)).wait_recv()
 
     def columns(t):
         return pl.ds(pl.multiple_of(t * T, T), T)
@@ -313,30 +318,34 @@
     for k in range(1, NX):
         xb_v[:, :, columns(lax.rem(x + k, NX))] = xg[:, k - 1].astype(BF16)
 
+    def rz_copy(h, k, src, slot, to):
+        return remote(dwp.at[h, src], rzr.at[h, slot], rz_ss.at[h, k], rz_rs.at[h, k], z_dev(to))
+
+    late = []
+
+    def half_product(h):
+        for t in range(NX):
+            k_t = gx[t, 4:6].reshape(T, DK).astype(BF16)
+            a_t = as_v[t, h * DK : (h + 1) * DK].astype(BF16)
+            vgs_v[t * T : (t + 1) * T] = (gx[t, 2 * h : 2 * h + 2].reshape(T, DK) + dot_nt(k_t, a_t)).astype(BF16)
+        dwp[h] = dot(xb_v[...].reshape(NZ * ROWS, NX * T), vgs_v[...]).reshape(NZ, ROWS, DK)
+        for k in (4, 3, 5, 2, 6, 1, 7):
+            t = lax.rem(z + k, NZ)
+            late.append(rz_copy(h, k, t, z, t))
+            late[-1].start()
+
     gx_wait((4,), (5,))
-    gx_wait((0, 1), (2, 3))
     x3_wait(0)
-
     acc = x3r[0].reshape(DV, DK)
     for t in (3, 2, 1, 0):
         as_v[t] = acc
-        k_t = gx[t, 4:6].reshape(T, DK).astype(BF16)
-        acc16 = acc.astype(BF16)
-        for h in range(2):
-            hl = slice(h * DK, (h + 1) * DK)
-            vgs_v[t * T : (t + 1) * T, hl] = (gx[t, 2 * h : 2 * h + 2].reshape(T, DK) + dot_nt(k_t, acc16[hl])).astype(BF16)
         if t:
             acc = slab_decay(0, t) * acc
-    dwp[...] = dot(xb_v[...].reshape(NZ * ROWS, NX * T), vgs_v[...]).reshape(NZ, ROWS, DV)
-
-    def rz_copy(k, src, slot, to):
-        return remote(dwp.at[src], rzr.at[slot], rz_ss.at[k], rz_rs.at[k], z_dev(to))
-
-    late = []
-    for k in (4, 3, 5, 2, 6, 1, 7):
-        t = lax.rem(z + k, NZ)
-        late.append(rz_copy(k, t, z, t))
-        late[-1].start()
+    gx_wait((0,), (1,))
+    half_product(0)
+    gx_forward((2,), (3,))
+    gx_wait((2,), (3,))
+    half_product(1)
     adj_in = adj_row + as_v[x]
     adj_in16 = adj_in.astype(BF16)
 
@@ -387,14 +396,16 @@
         def _():
             z_copy(1, k, z + k, z).wait_send()
 
-    total_dw = dwp[z]
-    for k in (1, 7, 2, 6, 3, 5, 4):
-        t = lax.rem(z + NZ - k, NZ)
-        rz_copy(k, t, t, t).wait_recv()
-        total_dw = total_dw + rzr[t]
-    dwo_v[...] = total_dw
-
-    squares = total_dw[:, :DK] * total_dw[:, :DK] + total_dw[:, DK:] * total_dw[:, DK:]
+    squares = jnp.zeros((ROWS, DK), F32)
+    for h in range(2):
+        part = dwp[h, z]
+        for k in (1, 7, 2, 6, 3, 5, 4):
+            t = lax.rem(z + NZ - k, NZ)
+            rz_copy(h, k, t, t, t).wait_recv()
+            part = part + rzr[h, t]
+        dwo_v[:, h * DK : (h + 1) * DK] = part
+        squares = squares + part * part
+
     norms = jnp.sum(squares.T, axis=0, keepdims=True)
     tps[...] = jnp.broadcast_to(jnp.concatenate([norms, jnp.zeros((1, 64), F32)], axis=1), (8, 128))
 
@@ -441,17 +452,17 @@
             vmem((2048, DV), BF16), vmem((T, DK), F32), vmem((T, DV), BF16),
             vmem((NX, NZ, ROWS, T), BF16), vmem((T, DV), BF16),
             vmem((NB, DV, DK), BF16), vmem((NB, DV, DK), BF16),
-            vmem((NX, DV, DK), F32), vmem((NX * T, DV), BF16), vmem((NZ, ROWS, NX * T), BF16),
+            vmem((NX, DV, DK), F32), vmem((NX * T, DK), BF16), vmem((NZ, ROWS, NX * T), BF16),
             vmem((2, NX, SLAB + 8, DK), F32), vmem((2, NX, SLAB + 8, DK), F32),
             vmem((2, SLAB + 8, DK), F32), vmem((2, NZ, SLAB + 8, DK), F32),
             vmem((NX, SLAB, DK), F32), vmem((NX, SLAB, DK), F32),
             vmem((2, NX, SLAB, DK), F32), vmem((2, NX, SLAB, DK), F32),
             vmem((NX, 6, T // 2, DK), F32), vmem((NX, ROWS, T), F32), vmem((NT, NX - 1, ROWS, T), F32),
-            vmem((NZ, ROWS, DV), F32), vmem((NZ, ROWS, DV), F32),
+            vmem((2, NZ, ROWS, DK), F32), vmem((2, NZ, ROWS, DK), F32),
             vmem((8, 128), F32), vmem((NT, 8, 128), F32),
             dma((6,)), dma((2, NX)), dma((2, NX)), dma((2, NZ)), dma((2, NZ)), dma((NX,)), dma((NX,)),
-            dma((2, NX)), dma((2, NX)), dma((4, 6)), dma((4, 6)), dma((NX,)), dma((NX,)), dma((NX,)), dma((NX,)),
-            dma((NX,)), dma((NX,)), dma((NZ,)), dma((NZ,)), dma((NT,)), dma((NT,)),
+            dma((2, NX)), dma((2, NX)), dma((4, 6)), dma((4, 6)), dma((NX,)), dma((NX,)), dma((NX, 3)), dma((NX, 3)),
+            dma((NX, 3)), dma((NX, 3)), dma((2, NZ)), dma((2, NZ)), dma((NT,)), dma((NT,)),
         ],
         compiler_params=pltpu.CompilerParams(collective_id=0, has_side_effects=True, vmem_limit_bytes=40 << 20),
         name="gla_backward",

time: 55.4 us -> 51.5 us (0.930)
  Pallas kernels: 54.7 us -> 50.7 us
    pallas_call x1, Pallas kernels: 53.9 us -> 49.9 us  [on_device(): pl.pallas_call(kernel, out_shape=tuple((vmem(*s) for s in shapes)), in_sp...]
where the time goes in v4:
time: 51.5 us; the launch traced here: 51.4 us
  Pallas kernels  50.7 us (98%)
  between operations  0.64 us (1%)
    pallas_call x1, Pallas kernels, on_device(): pl.pallas_call(kernel, out_shape=tuple((vmem(*s) for s in shapes)), in_sp...  49.9 us

profile of v4, /device:TPU:1, one launch (start us, length us, event | category | flops | bytes accessed | tf_op | source)
XLA Modules:
  0.0 51.4 jit_solution(16106784369919394556)
XLA Ops:
  0.6 49.9 %gla_backward.1 = (bf16[256,128]{1,0:T(8,128)(2,1)S(1)}, bf16[256,128]{1,0:T(8,128)(2,1)S(1)}, f32[256,128]{1,0:T(8,128)S(1)}, f32[64,256]{1,0:T(8,128)S(1)}, f32[1,64]{1,0:T(1,128)S(1)}) custom-call(bf16[256,2048]{1,0:T(8,128)(2,1)} %x_hbm.1, bf16[256,128]{1,0:T(8,128)(2,1)} %q_hbm.1, bf16[256,128]{1,0:T(8,128)(2,1)} %k_hbm.1, bf16[2048,256]{1,0:T(8,128)(2,1)} %w_hbm.1, ...), custom_call_target="tpu_custom_call" | custom-call | tf_op jit(solution)/shard_map/gla_backward/pallas_call | solution.py:445
  50.6 0.8 %finish.1 = (bf16[256,128]{1,0:T(8,128)(2,1)}, bf16[256,128]{1,0:T(8,128)(2,1)}, f32[256,128]{1,0:T(8,128)}, f32[64,256]{1,0:T(8,128)}, f32[1,64]{1,0:T(1,128)}) custom-call(bf16[256,128]{1,0:T(8,128)(2,1)S(1)} %get-tuple-element.15.refs_0_, bf16[256,128]{1,0:T(8,128)(2,1)S(1)} %get-tuple-element.16.refs_1_, f32[256,128]{1,0:T(8,128)S(1)} %get-tuple-element.17.refs_2_, ...), custom_call_target="tpu_custom_call" | custom-call | tf_op jit(solution)/shard_map/finish/pallas_call | solution.py:470

commit v5 on v4

--- a/solution.py
+++ b/solution.py
@@ -13,6 +13,7 @@
 NZ, NX, NT = 8, 4, 8
 SLAB = DV // NX
 ROWS = 64
+X1, Z2, XI, X3, GX, XX, XY, XC, RZ, TP = 0, 2, 3, 4, 6, 7, 8, 9, 10, 12
 MESH = pl.DeviceIdType.MESH
 F32, BF16 = jnp.float32, jnp.bfloat16
 
@@ -39,12 +40,11 @@
 
 def kernel(
     x_hbm, q_hbm, k_hbm, w_hbm, g_hbm, do_hbm,
-    dq_v, dk_v, dg_v, dwo_v, rn_v,
-    x_v, q_v, k_v, w_v, g_v, do_v,
+    dq_o, dk_o, dg_o, dwo_o, rn_o,
+    x_v, q_v, k_v, w_v, g_v, do_v, dq_v, dk_v, dg_v, dwo_v, rn_v,
     xt_v, val_v, locs_v, adjs_v, as_v, vgs_v, xb_v,
     x1s, x1r, z2s, z2r, xis, xir, x3s, x3r, gx, xts, xg, dwp, rzr, tps, tpr,
-    in_sem, x1_ss, x1_rs, z2_ss, z2_rs, xi_ss, xi_rs, x3_ss, x3_rs, gx_ss, gx_rs, xx_ss, xx_rs, xy_ss, xy_rs,
-    xc_ss, xc_rs, rz_ss, rz_rs, tp_ss, tp_rs,
+    in_sem, out_sem, sent, x1_rs, z2_rs, xi_rs, x3_rs, gx_rs, gx_rest, xx_rs, xy_rs, xc_rs, rz_rs, tp_rs,
 ):
     sp, tp = lax.axis_index("sp"), lax.axis_index("tp")
     z, x = sp // NX, lax.rem(sp, NX)
@@ -74,12 +74,6 @@
     ]
     for load in loads:
         load.start()
-
-    started = []
-
-    def go(cp):
-        cp.start()
-        started.append(cp)
 
     def remote(src, dst, ss, rs, dev):
         return pltpu.make_async_remote_copy(
@@ -153,53 +147,57 @@
         xts[t] = xt_v[t, tp].astype(F32)
     pl.semaphore_wait(barrier, NX - 1 + NZ - 1 + NT - 1)
 
-    def x1_copy(i, k, src, slot, to):
-        return remote(x1s.at[i, src], x1r.at[i, slot], x1_ss.at[i, k], x1_rs.at[i, k], x_dev(to))
+    def x1_copy(i, src, slot, to):
+        return remote(x1s.at[i, src], x1r.at[i, slot], sent.at[X1 + i], x1_rs.at[i], x_dev(to))
 
     def x_leg(i):
         for k in (2, 1, 3):
             t = lax.rem(x + k, NX)
-            go(x1_copy(i, k, t, x, t))
+            x1_copy(i, t, x, t).start()
         x1r[i, x] = x1s[i, x]
 
+    def arrived(ref, sem):
+        remote(ref, ref, sent.at[0], sem, x_dev(x)).wait_recv()
+
+    def left_here(ref, sem):
+        remote(ref, ref, sem, x1_rs.at[0], x_dev(x)).wait_send()
+
     def x_leg_wait(i):
-        for k in (2, 1, 3):
-            t = lax.rem(x + NX - k, NX)
-            x1_copy(i, k, t, t, t).wait_recv()
+        arrived(x1r.at[i, pl.ds(0, 3)], x1_rs.at[i])
 
     x_leg(0)
 
     def xx_copy(k, t):
-        return remote(xts.at[t], xg.at[tp, 3 - k], xx_ss.at[k], xx_rs.at[k], x_dev(t))
+        return remote(xts.at[t], xg.at[tp, 3 - k], sent.at[XX], xx_rs.at[k - 1], x_dev(t))
 
     for k in (1, 3, 2):
-        go(xx_copy(k, lax.rem(x + k, NX)))
+        xx_copy(k, lax.rem(x + k, NX)).start()
 
     right, left, far = lax.rem(x + 1, NX), lax.rem(x + 3, NX), lax.rem(x + 2, NX)
     ways = (right, left, right, left)
 
-    def gx_copy(kind, piece, slot):
+    def gx_copy(kind, piece, slot, sem):
         ref = gx.at[slot, piece]
-        return remote(ref, ref, gx_ss.at[kind, piece], gx_rs.at[kind, piece], x_dev(ways[kind]))
-
-    def gx_own(first, second):
-        for a, b in zip(first + second, second + first):
-            go(gx_copy(0, a, x))
-            go(gx_copy(1, b, x))
-
-    def gx_forward(first, second):
-        for a, b in zip(first, second):
-            gx_copy(0, a, left).wait_recv()
-            go(gx_copy(2, a, left))
-            gx_copy(1, b, right).wait_recv()
-            go(gx_copy(3, b, right))
-
-    def gx_wait(first, second):
-        for a, b in zip(first, second):
-            gx_copy(0, b, left).wait_recv()
-            gx_copy(1, a, right).wait_recv()
-            gx_copy(2, a, far).wait_recv()
-            gx_copy(3, b, far).wait_recv()
+        return remote(ref, ref, sent.at[GX], sem, x_dev(ways[kind]))
+
+    stages = ((4, 5), (0, 1), (2, 3))
+
+    def gx_own(stage):
+        a, b = stages[stage]
+        gx_copy(0, a, x, gx_rs.at[0, stage]).start()
+        gx_copy(1, b, x, gx_rs.at[1, stage]).start()
+        gx_copy(0, b, x, gx_rest.at[stage]).start()
+        gx_copy(1, a, x, gx_rest.at[stage]).start()
+
+    def gx_forward(stage):
+        a, b = stages[stage]
+        gx_copy(0, a, left, gx_rs.at[0, stage]).wait_recv()
+        gx_copy(2, a, left, gx_rest.at[stage]).start()
+        gx_copy(1, b, right, gx_rs.at[1, stage]).wait_recv()
+        gx_copy(3, b, right, gx_rest.at[stage]).start()
+
+    def gx_wait(stage):
+        arrived(gx.at[0, pl.ds(0, 4)], gx_rest.at[stage])
 
     loads[5].wait()
     val_v[...] = dot(x_v[...], w_v[...]).astype(BF16)
@@ -216,8 +214,8 @@
     def slab_decay(i, t):
         return x1r[i, t, SLAB : SLAB + 1, :]
 
-    def z_copy(i, k, t, slot):
-        return remote(z2s.at[i], z2r.at[i, slot], z2_ss.at[i, k], z2_rs.at[i, k], z_dev(t))
+    def z_copy(i, t, slot):
+        return remote(z2s.at[i], z2r.at[i, slot], sent.at[Z2], z2_rs.at[slot], z_dev(t))
 
     x_leg_wait(0)
     inner = [None] * NX
@@ -230,67 +228,63 @@
     for k in (4, 3, 5, 2, 6, 1, 7):
         @pl.when(z >= k)
         def _():
-            z_copy(0, k, z - k, z).start()
-
-    def xi_copy(k, src, slot, to):
-        return remote(xis.at[src], xir.at[slot], xi_ss.at[k], xi_rs.at[k], x_dev(to))
+            z_copy(0, z - k, z).start()
+
+    def xi_copy(src, slot, to):
+        return remote(xis.at[src], xir.at[slot], sent.at[XI], xi_rs.at[0], x_dev(to))
 
     for t in range(NX):
         xis[t] = inner[t]
     for k in (2, 1, 3):
         t = lax.rem(x + k, NX)
-        go(xi_copy(k, t, x, t))
+        xi_copy(t, x, t).start()
     xir[x] = xis[x]
-    gx_own((4,), (5,))
+    gx_own(0)
 
     sibling = tp + 1 - 2 * lax.rem(tp, 2)
 
     def xy_copy(j, k, slot, to):
         ref = xg.at[slot, k]
-        return remote(ref, ref, xy_ss.at[j, k], xy_rs.at[j, k], tp_dev(to))
-
-    def xc_copy(j, k, slot):
+        return remote(ref, ref, sent.at[XY], xy_rs.at[j - 1, k], tp_dev(to))
+
+    def xc_copy(k, slot):
         ref = xg.at[slot, k]
-        return remote(ref, ref, xc_ss.at[j, k], xc_rs.at[j, k], tp_dev(sibling))
+        return remote(ref, ref, sent.at[XC], xc_rs.at[0], tp_dev(sibling))
 
     for k in (1, 3, 2):
         xx_copy(k, lax.rem(x + NX - k, NX)).wait_recv()
         for j in (2, 1, 3):
-            go(xy_copy(j, 3 - k, tp, lax.rem(tp + 2 * j, NT)))
-        go(xc_copy(0, 3 - k, tp))
-
-    for k in (2, 1, 3):
-        t = lax.rem(x + NX - k, NX)
-        xi_copy(k, t, t, t).wait_recv()
+            xy_copy(j, 3 - k, tp, lax.rem(tp + 2 * j, NT)).start()
+        xc_copy(3 - k, tp).start()
+
+    arrived(xir.at[pl.ds(0, 3)], xi_rs.at[0])
     adj_row = xir[...].reshape(DV, DK)
     row_vg = local_vg + dot_nt(k_end.astype(BF16), adj_row.astype(BF16))
     for h in range(2):
         for p in range(2):
             gx[x, 2 * h + p] = row_vg[p * 128 : (p + 1) * 128, h * DK : (h + 1) * DK]
-    gx_own((0,), (1,))
-    gx_forward((4,), (5,))
+    gx_own(1)
+    gx_forward(0)
 
     def adj_step(n, acc):
         t = NZ - 1 - n
-        z_copy(0, t - z, t, t).wait_recv()
+        z_copy(0, t, t).wait_recv()
         return z2r[0, t, :SLAB, :] + z2r[0, t, SLAB : SLAB + 1, :] * acc
 
     x3s[0, 0] = lax.fori_loop(0, NZ - 1 - z, adj_step, jnp.zeros((SLAB, DK), F32))
 
-    def x3_copy(i, k, src, slot, to):
-        return remote(x3s.at[i, src], x3r.at[i, slot], x3_ss.at[i, k], x3_rs.at[i, k], x_dev(to))
+    def x3_copy(i, src, slot, to):
+        return remote(x3s.at[i, src], x3r.at[i, slot], sent.at[X3 + i], x3_rs.at[i], x_dev(to))
 
     def x3_wait(i):
-        for k in (2, 1, 3):
-            t = lax.rem(x + NX - k, NX)
-            x3_copy(i, k, 0, t, t).wait_recv()
+        arrived(x3r.at[i, pl.ds(0, 3)], x3_rs.at[i])
 
     for k in (2, 1, 3):
-        go(x3_copy(0, k, 0, x, lax.rem(x + k, NX)))
+        x3_copy(0, 0, x, lax.rem(x + k, NX)).start()
     x3r[0, x] = x3s[0, 0]
 
-    gx_forward((0,), (1,))
-    gx_own((2,), (3,))
+    gx_forward(1)
+    gx_own(2)
     x_leg_wait(1)
     acc = slab(1, 0)
     for t in range(1, NX):
@@ -300,16 +294,14 @@
     for k in (4, 3, 5, 2, 6, 1, 7):
         @pl.when(z + k < NZ)
         def _():
-            z_copy(1, k, z + k, z).start()
+            z_copy(1, z + k, z).start()
 
     for k in (1, 3, 2):
         for j in (1, 3, 2):
             slot = lax.rem(tp + NT - 2 * j, NT)
             xy_copy(j, 3 - k, slot, slot).wait_recv()
-            go(xc_copy(j, 3 - k, slot))
-    for j in (0, 1, 3, 2):
-        for k in (1, 3, 2):
-            xc_copy(j, 3 - k, lax.rem(sibling + NT - 2 * j, NT)).wait_recv()
+            xc_copy(3 - k, slot).start()
+    arrived(xg.at[pl.ds(0, 4)], xc_rs.at[0])
 
     def columns(t):
         return pl.ds(pl.multiple_of(t * T, T), T)
@@ -318,10 +310,8 @@
     for k in range(1, NX):
         xb_v[:, :, columns(lax.rem(x + k, NX))] = xg[:, k - 1].astype(BF16)
 
-    def rz_copy(h, k, src, slot, to):
-        return remote(dwp.at[h, src], rzr.at[h, slot], rz_ss.at[h, k], rz_rs.at[h, k], z_dev(to))
-
-    late = []
+    def rz_copy(h, src, slot, to):
+        return remote(dwp.at[h, src], rzr.at[h, slot], sent.at[RZ + h], rz_rs.at[h], z_dev(to))
 
     def half_product(h):
         for t in range(NX):
@@ -331,20 +321,19 @@
         dwp[h] = dot(xb_v[...].reshape(NZ * ROWS, NX * T), vgs_v[...]).reshape(NZ, ROWS, DK)
         for k in (4, 3, 5, 2, 6, 1, 7):
             t = lax.rem(z + k, NZ)
-            late.append(rz_copy(h, k, t, z, t))
-            late[-1].start()
-
-    gx_wait((4,), (5,))
+            rz_copy(h, t, z, t).start()
+
+    gx_wait(0)
     x3_wait(0)
     acc = x3r[0].reshape(DV, DK)
     for t in (3, 2, 1, 0):
         as_v[t] = acc
         if t:
             acc = slab_decay(0, t) * acc
-    gx_wait((0,), (1,))
+    gx_wait(1)
     half_product(0)
-    gx_forward((2,), (3,))
-    gx_wait((2,), (3,))
+    gx_forward(2)
+    gx_wait(2)
     half_product(1)
     adj_in = adj_row + as_v[x]
     adj_in16 = adj_in.astype(BF16)
@@ -367,7 +356,7 @@
     dk_v[...] = kg.astype(BF16)
 
     def state_step(t, acc):
-        z_copy(1, z - t, t, t).wait_recv()
+        z_copy(1, t, t).wait_recv()
         return z2r[1, t, :SLAB, :] + z2r[1, t, SLAB : SLAB + 1, :] * acc
 
     acc = lax.fori_loop(0, z, state_step, jnp.zeros((SLAB, DK), F32))
@@ -377,7 +366,7 @@
             acc = slab(1, t) + slab_decay(1, t) * acc
     for k in (2, 1, 3):
         t = lax.rem(x + k, NX)
-        go(x3_copy(1, k, t, x, t))
+        x3_copy(1, t, x, t).start()
     x3r[1, x] = x3s[1, x]
     x3_wait(1)
     state_in = x3r[1].reshape(DV, DK)
@@ -385,44 +374,56 @@
     dq_v[...] = (qg * (DK**-0.5)).astype(BF16)
     carry = jnp.sum(adj_in * (span_state + span_decay * state_in), axis=0, keepdims=True)
     dg_v[...] = exact_sum((col >= row).astype(BF16), qs * qg - kf * kg) + carry
-    for cp in started:
-        cp.wait_send()
-    for k in range(1, NZ):
-        @pl.when(z >= k)
-        def _():
-            z_copy(0, k, z - k, z).wait_send()
-
-        @pl.when(z + k < NZ)
-        def _():
-            z_copy(1, k, z + k, z).wait_send()
+    stores = [
+        pltpu.make_async_copy(src, dst, out_sem.at[i])
+        for i, (src, dst) in enumerate(((dq_v, dq_o), (dk_v, dk_o), (dg_v, dg_o), (dwo_v, dwo_o), (rn_v, rn_o)))
+    ]
+    for store in stores[:3]:
+        store.start()
+
+    left_here(x1s.at[0, pl.ds(0, 3)], sent.at[X1])
+    left_here(x1s.at[1, pl.ds(0, 3)], sent.at[X1 + 1])
+    left_here(z2r.at[0, pl.ds(0, 7)], sent.at[Z2])
+    left_here(xis.at[pl.ds(0, 3)], sent.at[XI])
+    left_here(x3r.at[0, pl.ds(0, 3)], sent.at[X3])
+    left_here(x3r.at[1, pl.ds(0, 3)], sent.at[X3 + 1])
+    left_here(gx.at[pl.ds(0, 3)], sent.at[GX])
+    left_here(xts.at[pl.ds(0, 3)], sent.at[XX])
+    left_here(xg.at[pl.ds(0, 3)], sent.at[XY])
+    left_here(xg.at[pl.ds(0, 4)], sent.at[XC])
+    for store in stores[:3]:
+        store.wait()
 
     squares = jnp.zeros((ROWS, DK), F32)
     for h in range(2):
         part = dwp[h, z]
-        for k in (1, 7, 2, 6, 3, 5, 4):
-            t = lax.rem(z + NZ - k, NZ)
-            rz_copy(h, k, t, t, t).wait_recv()
-            part = part + rzr[h, t]
+        arrived(rzr.at[h, pl.ds(0, 7)], rz_rs.at[h])
+        for k in range(1, NZ):
+            part = part + rzr[h, lax.rem(z + k, NZ)]
         dwo_v[:, h * DK : (h + 1) * DK] = part
         squares = squares + part * part
+    stores[3].start()
 
     norms = jnp.sum(squares.T, axis=0, keepdims=True)
     tps[...] = jnp.broadcast_to(jnp.concatenate([norms, jnp.zeros((1, 64), F32)], axis=1), (8, 128))
 
-    def tp_copy(k, slot, to):
-        return remote(tps, tpr.at[slot], tp_ss.at[k], tp_rs.at[k], tp_dev(to))
+    def tp_copy(slot, to):
+        return remote(tps, tpr.at[slot], sent.at[TP], tp_rs.at[0], tp_dev(to))
 
     for k in range(1, NT):
-        late.append(tp_copy(k, tp, lax.rem(tp + k, NT)))
-        late[-1].start()
+        tp_copy(tp, lax.rem(tp + k, NT)).start()
+    left_here(dwp.at[0, pl.ds(0, 7)], sent.at[RZ])
+    left_here(dwp.at[1, pl.ds(0, 7)], sent.at[RZ + 1])
+    stores[3].wait()
+    left_here(tpr.at[pl.ds(0, 7)], sent.at[TP])
+    arrived(tpr.at[pl.ds(0, 7)], tp_rs.at[0])
     acc = tps[0:1, :]
     for k in range(1, NT):
         t = lax.rem(tp + NT - k, NT)
-        tp_copy(k, t, t).wait_recv()
         acc = acc + tpr[t, 0:1, :]
     rn_v[...] = acc[:, :ROWS]
-    for cp in late:
-        cp.wait_send()
+    stores[4].start()
+    stores[4].wait()
 
 
 def finish(*refs):
@@ -436,7 +437,7 @@
 
 def on_device(block_input, queries, keys, w_value, log_decay, d_out):
     dma, vmem = pltpu.SemaphoreType.DMA, pltpu.VMEM
-    hbm_spec, vmem_spec = pl.BlockSpec(memory_space=pltpu.HBM), pl.BlockSpec(memory_space=vmem)
+    hbm_spec = pl.BlockSpec(memory_space=pltpu.HBM)
     shapes = (((T, DK), BF16), ((T, DK), BF16), ((T, DK), F32), ((ROWS, DV), F32), ((1, ROWS), F32))
     args = [
         pltpu.with_memory_space_constraint(a, pltpu.HBM)
@@ -446,10 +447,12 @@
         kernel,
         out_shape=tuple(vmem(*s) for s in shapes),
         in_specs=[hbm_spec] * 6,
-        out_specs=(vmem_spec,) * 5,
+        out_specs=(pl.BlockSpec(memory_space=pl.ANY),) * 5,
         scratch_shapes=[
             vmem((T, 2048), BF16), vmem((T, DK), BF16), vmem((T, DK), BF16),
             vmem((2048, DV), BF16), vmem((T, DK), F32), vmem((T, DV), BF16),
+            vmem((T, DK), BF16), vmem((T, DK), BF16), vmem((T, DK), F32),
+            vmem((ROWS, DV), F32), vmem((1, ROWS), F32),
             vmem((NX, NZ, ROWS, T), BF16), vmem((T, DV), BF16),
             vmem((NB, DV, DK), BF16), vmem((NB, DV, DK), BF16),
             vmem((NX, DV, DK), F32), vmem((NX * T, DK), BF16), vmem((NZ, ROWS, NX * T), BF16),
@@ -460,9 +463,8 @@
             vmem((NX, 6, T // 2, DK), F32), vmem((NX, ROWS, T), F32), vmem((NT, NX - 1, ROWS, T), F32),
             vmem((2, NZ, ROWS, DK), F32), vmem((2, NZ, ROWS, DK), F32),
             vmem((8, 128), F32), vmem((NT, 8, 128), F32),
-            dma((6,)), dma((2, NX)), dma((2, NX)), dma((2, NZ)), dma((2, NZ)), dma((NX,)), dma((NX,)),
-            dma((2, NX)), dma((2, NX)), dma((4, 6)), dma((4, 6)), dma((NX,)), dma((NX,)), dma((NX, 3)), dma((NX, 3)),
-            dma((NX, 3)), dma((NX, 3)), dma((2, NZ)), dma((2, NZ)), dma((NT,)), dma((NT,)),
+            dma((6,)), dma((5,)), dma((13,)), dma((2,)), dma((NZ,)), dma((1,)), dma((2,)), dma((2, 3)), dma((3,)),
+            dma((3,)), dma((3, 3)), dma((1,)), dma((2,)), dma((1,)),
         ],
         compiler_params=pltpu.CompilerParams(collective_id=0, has_side_effects=True, vmem_limit_bytes=40 << 20),
         name="gla_backward",

time: 51.5 us -> 50 us (0.971)
  Pallas kernels: 50.7 us -> 49.3 us
    pallas_call x1, Pallas kernels: 49.9 us -> 48.5 us  [on_device(): pl.pallas_call(kernel, out_shape=tuple((vmem(*s) for s in shapes)), in_sp...]
where the time goes in v5:
time: 50 us; the launch traced here: 49.9 us
  Pallas kernels  49.3 us (99%)
  between operations  0.64 us (1%)
    pallas_call x1, Pallas kernels, on_device(): pl.pallas_call(kernel, out_shape=tuple((vmem(*s) for s in shapes)), in_sp...  48.5 us

profile of v5, /device:TPU:1, one launch (start us, length us, event | category | flops | bytes accessed | tf_op | source)
XLA Modules:
  0.0 49.9 jit_solution(7601995387382473311)
XLA Ops:
  0.6 48.5 %gla_backward.1 = (bf16[256,128]{1,0:T(8,128)(2,1)S(1)}, bf16[256,128]{1,0:T(8,128)(2,1)S(1)}, f32[256,128]{1,0:T(8,128)S(1)}, f32[64,256]{1,0:T(8,128)S(1)}, f32[1,64]{1,0:T(1,128)S(1)}) custom-call(bf16[256,2048]{1,0:T(8,128)(2,1)} %x_hbm.1, bf16[256,128]{1,0:T(8,128)(2,1)} %q_hbm.1, bf16[256,128]{1,0:T(8,128)(2,1)} %k_hbm.1, bf16[2048,256]{1,0:T(8,128)(2,1)} %w_hbm.1, ...), custom_call_target="tpu_custom_call" | custom-call | tf_op jit(solution)/shard_map/gla_backward/pallas_call | solution.py:446
  49.2 0.8 %finish.1 = (bf16[256,128]{1,0:T(8,128)(2,1)}, bf16[256,128]{1,0:T(8,128)(2,1)}, f32[256,128]{1,0:T(8,128)}, f32[64,256]{1,0:T(8,128)}, f32[1,64]{1,0:T(1,128)}) custom-call(bf16[256,128]{1,0:T(8,128)(2,1)S(1)} %get-tuple-element.15.refs_0_, bf16[256,128]{1,0:T(8,128)(2,1)S(1)} %get-tuple-element.16.refs_1_, f32[256,128]{1,0:T(8,128)S(1)} %get-tuple-element.17.refs_2_, ...), custom_call_target="tpu_custom_call" | custom-call | tf_op jit(solution)/shard_map/finish/pallas_call | solution.py:472

commit v6 on v5

--- a/solution.py
+++ b/solution.py
@@ -42,9 +42,9 @@
     x_hbm, q_hbm, k_hbm, w_hbm, g_hbm, do_hbm,
     dq_o, dk_o, dg_o, dwo_o, rn_o,
     x_v, q_v, k_v, w_v, g_v, do_v, dq_v, dk_v, dg_v, dwo_v, rn_v,
-    xt_v, val_v, locs_v, adjs_v, as_v, vgs_v, xb_v,
+    xt_v, val_v, locs_v, adjs_v, as_v, xb_v,
     x1s, x1r, z2s, z2r, xis, xir, x3s, x3r, gx, xts, xg, dwp, rzr, tps, tpr,
-    in_sem, out_sem, sent, x1_rs, z2_rs, xi_rs, x3_rs, gx_rs, gx_rest, xx_rs, xy_rs, xc_rs, rz_rs, tp_rs,
+    in_sem, out_sem, sent, x1_rs, z2_rs, xi_rs, x3_rs, gx_rs, gx_rest, gx_far, xx_rs, xy_rs, xc_rs, rz_rs, tp_rs,
 ):
     sp, tp = lax.axis_index("sp"), lax.axis_index("tp")
     z, x = sp // NX, lax.rem(sp, NX)
@@ -117,6 +117,66 @@
     for s in range(NX):
         x1s[0, s, :SLAB, :] = span_adj[s * SLAB : (s + 1) * SLAB]
         x1s[0, s, SLAB:, :] = wide_decay
+
+    pl.semaphore_wait(barrier, NX - 1 + NZ - 1 + NT - 1)
+
+    def x1_copy(i, src, slot, to):
+        return remote(x1s.at[i, src], x1r.at[i, slot], sent.at[X1 + i], x1_rs.at[i], x_dev(to))
+
+    def x_leg(i):
+        for k in (2, 1, 3):
+            t = lax.rem(x + k, NX)
+            x1_copy(i, t, x, t).start()
+        x1r[i, x] = x1s[i, x]
+
+    def arrived(ref, sem):
+        remote(ref, ref, sent.at[0], sem, x_dev(x)).wait_recv()
+
+    def left_here(ref, sem):
+        remote(ref, ref, sem, x1_rs.at[0], x_dev(x)).wait_send()
+
+    def x_leg_wait(i):
+        arrived(x1r.at[i, pl.ds(0, 3)], x1_rs.at[i])
+
+    x_leg(0)
+
+    loads[4].wait()
+    for zz in range(NZ):
+        xt_v[:, zz] = x_v[:, zz * NX * ROWS : (zz + 1) * NX * ROWS].T.reshape(NX, ROWS, T)
+    for t in range(NX):
+        xts[t] = xt_v[t, tp].astype(F32)
+
+    def xx_copy(k, t):
+        return remote(xts.at[t], xg.at[tp, 3 - k], sent.at[XX], xx_rs.at[k - 1], x_dev(t))
+
+    for k in (1, 3, 2):
+        xx_copy(k, lax.rem(x + k, NX)).start()
+
+    right, left, far = lax.rem(x + 1, NX), lax.rem(x + 3, NX), lax.rem(x + 2, NX)
+    ways = (right, left, right, left)
+
+    def gx_copy(kind, piece, slot, sem):
+        ref = gx.at[slot, piece]
+        return remote(ref, ref, sent.at[GX], sem, x_dev(ways[kind]))
+
+    stages = ((4, 5), (0, 1), (2, 3))
+
+    def gx_own(stage):
+        a, b = stages[stage]
+        gx_copy(0, a, x, gx_rs.at[0, stage]).start()
+        gx_copy(1, b, x, gx_rs.at[1, stage]).start()
+        gx_copy(0, b, x, gx_rest.at[stage]).start()
+        gx_copy(1, a, x, gx_rest.at[stage]).start()
+
+    def gx_forward(stage):
+        a, b = stages[stage]
+        gx_copy(0, a, left, gx_rs.at[0, stage]).wait_recv()
+        gx_copy(2, a, left, gx_far.at[stage]).start()
+        gx_copy(1, b, right, gx_rs.at[1, stage]).wait_recv()
+        gx_copy(3, b, right, gx_far.at[stage]).start()
+
+    def gx_wait(sems, stage):
+        arrived(gx.at[0, pl.ds(0, 2)], sems.at[stage])
 
     loads[3].wait()
     kf = k_v[...].astype(F32)
@@ -140,65 +200,6 @@
     gx[x, 4] = k_end[: T // 2]
     gx[x, 5] = k_end[T // 2 :]
 
-    loads[4].wait()
-    for zz in range(NZ):
-        xt_v[:, zz] = x_v[:, zz * NX * ROWS : (zz + 1) * NX * ROWS].T.reshape(NX, ROWS, T)
-    for t in range(NX):
-        xts[t] = xt_v[t, tp].astype(F32)
-    pl.semaphore_wait(barrier, NX - 1 + NZ - 1 + NT - 1)
-
-    def x1_copy(i, src, slot, to):
-        return remote(x1s.at[i, src], x1r.at[i, slot], sent.at[X1 + i], x1_rs.at[i], x_dev(to))
-
-    def x_leg(i):
-        for k in (2, 1, 3):
-            t = lax.rem(x + k, NX)
-            x1_copy(i, t, x, t).start()
-        x1r[i, x] = x1s[i, x]
-
-    def arrived(ref, sem):
-        remote(ref, ref, sent.at[0], sem, x_dev(x)).wait_recv()
-
-    def left_here(ref, sem):
-        remote(ref, ref, sem, x1_rs.at[0], x_dev(x)).wait_send()
-
-    def x_leg_wait(i):
-        arrived(x1r.at[i, pl.ds(0, 3)], x1_rs.at[i])
-
-    x_leg(0)
-
-    def xx_copy(k, t):
-        return remote(xts.at[t], xg.at[tp, 3 - k], sent.at[XX], xx_rs.at[k - 1], x_dev(t))
-
-    for k in (1, 3, 2):
-        xx_copy(k, lax.rem(x + k, NX)).start()
-
-    right, left, far = lax.rem(x + 1, NX), lax.rem(x + 3, NX), lax.rem(x + 2, NX)
-    ways = (right, left, right, left)
-
-    def gx_copy(kind, piece, slot, sem):
-        ref = gx.at[slot, piece]
-        return remote(ref, ref, sent.at[GX], sem, x_dev(ways[kind]))
-
-    stages = ((4, 5), (0, 1), (2, 3))
-
-    def gx_own(stage):
-        a, b = stages[stage]
-        gx_copy(0, a, x, gx_rs.at[0, stage]).start()
-        gx_copy(1, b, x, gx_rs.at[1, stage]).start()
-        gx_copy(0, b, x, gx_rest.at[stage]).start()
-        gx_copy(1, a, x, gx_rest.at[stage]).start()
-
-    def gx_forward(stage):
-        a, b = stages[stage]
-        gx_copy(0, a, left, gx_rs.at[0, stage]).wait_recv()
-        gx_copy(2, a, left, gx_rest.at[stage]).start()
-        gx_copy(1, b, right, gx_rs.at[1, stage]).wait_recv()
-        gx_copy(3, b, right, gx_rest.at[stage]).start()
-
-    def gx_wait(stage):
-        arrived(gx.at[0, pl.ds(0, 4)], gx_rest.at[stage])
-
     loads[5].wait()
     val_v[...] = dot(x_v[...], w_v[...]).astype(BF16)
     v = val_v[...]
@@ -313,27 +314,31 @@
     def rz_copy(h, src, slot, to):
         return remote(dwp.at[h, src], rzr.at[h, slot], sent.at[RZ + h], rz_rs.at[h], z_dev(to))
 
+    def product(h, t):
+        k_t = gx[t, 4:6].reshape(T, DK).astype(BF16)
+        a_t = as_v[t, h * DK : (h + 1) * DK].astype(BF16)
+        vg = (gx[t, 2 * h : 2 * h + 2].reshape(T, DK) + dot_nt(k_t, a_t)).astype(BF16)
+        return dot(xb_v[:, :, columns(t)].reshape(NZ * ROWS, T), vg)
+
     def half_product(h):
-        for t in range(NX):
-            k_t = gx[t, 4:6].reshape(T, DK).astype(BF16)
-            a_t = as_v[t, h * DK : (h + 1) * DK].astype(BF16)
-            vgs_v[t * T : (t + 1) * T] = (gx[t, 2 * h : 2 * h + 2].reshape(T, DK) + dot_nt(k_t, a_t)).astype(BF16)
-        dwp[h] = dot(xb_v[...].reshape(NZ * ROWS, NX * T), vgs_v[...]).reshape(NZ, ROWS, DK)
+        gx_wait(gx_rest, h + 1)
+        near = product(h, x) + product(h, left) + product(h, right)
+        gx_wait(gx_far, h + 1)
+        dwp[h] = (near + product(h, far)).reshape(NZ, ROWS, DK)
         for k in (4, 3, 5, 2, 6, 1, 7):
             t = lax.rem(z + k, NZ)
             rz_copy(h, t, z, t).start()
 
-    gx_wait(0)
+    gx_wait(gx_rest, 0)
+    gx_wait(gx_far, 0)
     x3_wait(0)
     acc = x3r[0].reshape(DV, DK)
     for t in (3, 2, 1, 0):
         as_v[t] = acc
         if t:
             acc = slab_decay(0, t) * acc
-    gx_wait(1)
     half_product(0)
     gx_forward(2)
-    gx_wait(2)
     half_product(1)
     adj_in = adj_row + as_v[x]
     adj_in16 = adj_in.astype(BF16)
@@ -455,7 +460,7 @@
             vmem((ROWS, DV), F32), vmem((1, ROWS), F32),
             vmem((NX, NZ, ROWS, T), BF16), vmem((T, DV), BF16),
             vmem((NB, DV, DK), BF16), vmem((NB, DV, DK), BF16),
-            vmem((NX, DV, DK), F32), vmem((NX * T, DK), BF16), vmem((NZ, ROWS, NX * T), BF16),
+            vmem((NX, DV, DK), F32), vmem((NZ, ROWS, NX * T), BF16),
             vmem((2, NX, SLAB + 8, DK), F32), vmem((2, NX, SLAB + 8, DK), F32),
             vmem((2, SLAB + 8, DK), F32), vmem((2, NZ, SLAB + 8, DK), F32),
             vmem((NX, SLAB, DK), F32), vmem((NX, SLAB, DK), F32),
@@ -464,7 +469,7 @@
             vmem((2, NZ, ROWS, DK), F32), vmem((2, NZ, ROWS, DK), F32),
             vmem((8, 128), F32), vmem((NT, 8, 128), F32),
             dma((6,)), dma((5,)), dma((13,)), dma((2,)), dma((NZ,)), dma((1,)), dma((2,)), dma((2, 3)), dma((3,)),
-            dma((3,)), dma((3, 3)), dma((1,)), dma((2,)), dma((1,)),
+            dma((3,)), dma((3,)), dma((3, 3)), dma((1,)), dma((2,)), dma((1,)),
         ],
         compiler_params=pltpu.CompilerParams(collective_id=0, has_side_effects=True, vmem_limit_bytes=40 << 20),
         name="gla_backward",

time: 50 us -> 48.5 us (0.970)
  Pallas kernels: 49.3 us -> 47.8 us
    pallas_call x1, Pallas kernels: 48.5 us -> 47 us  [on_device(): pl.pallas_call(kernel, out_shape=tuple((vmem(*s) for s in shapes)), in_sp...]
where the time goes in v6:
time: 48.5 us; the launch traced here: 48.4 us
  Pallas kernels  47.8 us (99%)
  between operations  0.64 us (1%)
    pallas_call x1, Pallas kernels, on_device(): pl.pallas_call(kernel, out_shape=tuple((vmem(*s) for s in shapes)), in_sp...  47 us

profile of v6, /device:TPU:1, one launch (start us, length us, event | category | flops | bytes accessed | tf_op | source)
XLA Modules:
  0.0 48.4 jit_solution(8973337875869425908)
XLA Ops:
  0.6 47.0 %gla_backward.1 = (bf16[256,128]{1,0:T(8,128)(2,1)S(1)}, bf16[256,128]{1,0:T(8,128)(2,1)S(1)}, f32[256,128]{1,0:T(8,128)S(1)}, f32[64,256]{1,0:T(8,128)S(1)}, f32[1,64]{1,0:T(1,128)S(1)}) custom-call(bf16[256,2048]{1,0:T(8,128)(2,1)} %x_hbm.1, bf16[256,128]{1,0:T(8,128)(2,1)} %q_hbm.1, bf16[256,128]{1,0:T(8,128)(2,1)} %k_hbm.1, bf16[2048,256]{1,0:T(8,128)(2,1)} %w_hbm.1, ...), custom_call_target="tpu_custom_call" | custom-call | tf_op jit(solution)/shard_map/gla_backward/pallas_call | solution.py:451
  47.7 0.8 %finish.1 = (bf16[256,128]{1,0:T(8,128)(2,1)}, bf16[256,128]{1,0:T(8,128)(2,1)}, f32[256,128]{1,0:T(8,128)}, f32[64,256]{1,0:T(8,128)}, f32[1,64]{1,0:T(1,128)}) custom-call(bf16[256,128]{1,0:T(8,128)(2,1)S(1)} %get-tuple-element.15.refs_0_, bf16[256,128]{1,0:T(8,128)(2,1)S(1)} %get-tuple-element.16.refs_1_, f32[256,128]{1,0:T(8,128)S(1)} %get-tuple-element.17.refs_2_, ...), custom_call_target="tpu_custom_call" | custom-call | tf_op jit(solution)/shard_map/finish/pallas_call | solution.py:477

commit v7 on v6

--- a/solution.py
+++ b/solution.py
@@ -58,21 +58,23 @@
     def tp_dev(t):
         return {"tp": t}
 
-    barrier = pltpu.get_barrier_semaphore()
-    for k in range(1, NX):
-        pl.semaphore_signal(barrier, inc=1, device_id=x_dev(lax.rem(x + k, NX)), device_id_type=MESH)
-    for k in range(1, NZ):
-        pl.semaphore_signal(barrier, inc=1, device_id=z_dev(lax.rem(z + k, NZ)), device_id_type=MESH)
-    for k in range(1, NT):
-        pl.semaphore_signal(barrier, inc=1, device_id=tp_dev(lax.rem(tp + k, NT)), device_id_type=MESH)
-
     loads = [
         pltpu.make_async_copy(src, dst, in_sem.at[i])
         for i, (src, dst) in enumerate(
             ((g_hbm, g_v), (q_hbm, q_v), (do_hbm, do_v), (k_hbm, k_v), (x_hbm, x_v), (w_hbm, w_v))
         )
     ]
-    for load in loads:
+    for load in loads[:3]:
+        load.start()
+
+    barrier = pltpu.get_barrier_semaphore()
+    for k in (4, 3, 5, 2, 6, 1, 7):
+        pl.semaphore_signal(barrier, inc=1, device_id=z_dev(lax.rem(z + k, NZ)), device_id_type=MESH)
+    for k in (2, 1, 3):
+        pl.semaphore_signal(barrier, inc=1, device_id=x_dev(lax.rem(x + k, NX)), device_id_type=MESH)
+    for k in range(1, NT):
+        pl.semaphore_signal(barrier, inc=1, device_id=tp_dev(lax.rem(tp + k, NT)), device_id_type=MESH)
+    for load in loads[3:]:
         load.start()
 
     def remote(src, dst, ss, rs, dev):
@@ -121,7 +123,8 @@
     pl.semaphore_wait(barrier, NX - 1 + NZ - 1 + NT - 1)
 
     def x1_copy(i, src, slot, to):
-        return remote(x1s.at[i, src], x1r.at[i, slot], sent.at[X1 + i], x1_rs.at[i], x_dev(to))
+        rows = pl.ds(0, SLAB + 8 * (1 - i))
+        return remote(x1s.at[i, src, rows], x1r.at[i, slot, rows], sent.at[X1 + i], x1_rs.at[i], x_dev(to))
 
     def x_leg(i):
         for k in (2, 1, 3):
@@ -136,7 +139,7 @@
         remote(ref, ref, sem, x1_rs.at[0], x_dev(x)).wait_send()
 
     def x_leg_wait(i):
-        arrived(x1r.at[i, pl.ds(0, 3)], x1_rs.at[i])
+        arrived(x1r.at[i, pl.ds(0, 3), pl.ds(0, SLAB + 8 * (1 - i))], x1_rs.at[i])
 
     x_leg(0)
 
@@ -155,25 +158,32 @@
     right, left, far = lax.rem(x + 1, NX), lax.rem(x + 3, NX), lax.rem(x + 2, NX)
     ways = (right, left, right, left)
 
-    def gx_copy(kind, piece, slot, sem):
-        ref = gx.at[slot, piece]
+    def gx_copy(kind, piece, slot, sem, rows):
+        ref = gx.at[slot, piece, rows]
         return remote(ref, ref, sent.at[GX], sem, x_dev(ways[kind]))
 
     stages = ((4, 5), (0, 1), (2, 3))
+
+    def cuts(stage):
+        n = 2 if stage == 2 else 1
+        return [(stage + i, pl.ds(i * (T // 2 // n), T // 2 // n)) for i in range(n)]
 
     def gx_own(stage):
         a, b = stages[stage]
-        gx_copy(0, a, x, gx_rs.at[0, stage]).start()
-        gx_copy(1, b, x, gx_rs.at[1, stage]).start()
-        gx_copy(0, b, x, gx_rest.at[stage]).start()
-        gx_copy(1, a, x, gx_rest.at[stage]).start()
+        for n, rows in cuts(stage):
+            gx_copy(0, a, x, gx_rs.at[0, n], rows).start()
+            gx_copy(1, b, x, gx_rs.at[1, n], rows).start()
+        whole = pl.ds(0, T // 2)
+        gx_copy(0, b, x, gx_rest.at[stage], whole).start()
+        gx_copy(1, a, x, gx_rest.at[stage], whole).start()
 
     def gx_forward(stage):
         a, b = stages[stage]
-        gx_copy(0, a, left, gx_rs.at[0, stage]).wait_recv()
-        gx_copy(2, a, left, gx_far.at[stage]).start()
-        gx_copy(1, b, right, gx_rs.at[1, stage]).wait_recv()
-        gx_copy(3, b, right, gx_far.at[stage]).start()
+        for n, rows in cuts(stage):
+            gx_copy(0, a, left, gx_rs.at[0, n], rows).wait_recv()
+            gx_copy(2, a, left, gx_far.at[stage], rows).start()
+            gx_copy(1, b, right, gx_rs.at[1, n], rows).wait_recv()
+            gx_copy(3, b, right, gx_far.at[stage], rows).start()
 
     def gx_wait(sems, stage):
         arrived(gx.at[0, pl.ds(0, 2)], sems.at[stage])
@@ -289,7 +299,7 @@
     x_leg_wait(1)
     acc = slab(1, 0)
     for t in range(1, NX):
-        acc = slab(1, t) + slab_decay(1, t) * acc
+        acc = slab(1, t) + slab_decay(0, t) * acc
     z2s[1, :SLAB, :] = acc
     z2s[1, SLAB:, :] = jnp.broadcast_to(row_decay, (8, DK))
     for k in (4, 3, 5, 2, 6, 1, 7):
@@ -368,7 +378,7 @@
     for t in range(NX):
         x3s[1, t] = acc
         if t < NX - 1:
-            acc = slab(1, t) + slab_decay(1, t) * acc
+            acc = slab(1, t) + slab_decay(0, t) * acc
     for k in (2, 1, 3):
         t = lax.rem(x + k, NX)
         x3_copy(1, t, x, t).start()
@@ -387,7 +397,7 @@
         store.start()
 
     left_here(x1s.at[0, pl.ds(0, 3)], sent.at[X1])
-    left_here(x1s.at[1, pl.ds(0, 3)], sent.at[X1 + 1])
+    left_here(x1s.at[1, pl.ds(0, 3), pl.ds(0, SLAB)], sent.at[X1 + 1])
     left_here(z2r.at[0, pl.ds(0, 7)], sent.at[Z2])
     left_here(xis.at[pl.ds(0, 3)], sent.at[XI])
     left_here(x3r.at[0, pl.ds(0, 3)], sent.at[X3])
@@ -468,7 +478,7 @@
             vmem((NX, 6, T // 2, DK), F32), vmem((NX, ROWS, T), F32), vmem((NT, NX - 1, ROWS, T), F32),
             vmem((2, NZ, ROWS, DK), F32), vmem((2, NZ, ROWS, DK), F32),
             vmem((8, 128), F32), vmem((NT, 8, 128), F32),
-            dma((6,)), dma((5,)), dma((13,)), dma((2,)), dma((NZ,)), dma((1,)), dma((2,)), dma((2, 3)), dma((3,)),
+            dma((6,)), dma((5,)), dma((13,)), dma((2,)), dma((NZ,)), dma((1,)), dma((2,)), dma((2, 4)), dma((3,)),
             dma((3,)), dma((3,)), dma((3, 3)), dma((1,)), dma((2,)), dma((1,)),
         ],
         compiler_params=pltpu.CompilerParams(collective_id=0, has_side_effects=True, vmem_limit_bytes=40 << 20),

time: 48.5 us -> 48.3 us (level)
  no operation moved by 1% of the time
where the time goes in v7:
time: 48.3 us; the launch traced here: 48.2 us
  Pallas kernels  47.5 us (98%)
  between operations  0.64 us (1%)
    pallas_call x1, Pallas kernels, on_device(): pl.pallas_call(kernel, out_shape=tuple((vmem(*s) for s in shapes)), in_sp...  46.8 us

profile of v7, /device:TPU:1, one launch (start us, length us, event | category | flops | bytes accessed | tf_op | source)
XLA Modules:
  0.0 48.2 jit_solution(3563827786819935039)
XLA Ops:
  0.6 46.8 %gla_backward.1 = (bf16[256,128]{1,0:T(8,128)(2,1)S(1)}, bf16[256,128]{1,0:T(8,128)(2,1)S(1)}, f32[256,128]{1,0:T(8,128)S(1)}, f32[64,256]{1,0:T(8,128)S(1)}, f32[1,64]{1,0:T(1,128)S(1)}) custom-call(bf16[256,2048]{1,0:T(8,128)(2,1)} %x_hbm.1, bf16[256,128]{1,0:T(8,128)(2,1)} %q_hbm.1, bf16[256,128]{1,0:T(8,128)(2,1)} %k_hbm.1, bf16[2048,256]{1,0:T(8,128)(2,1)} %w_hbm.1, ...), custom_call_target="tpu_custom_call" | custom-call | tf_op jit(solution)/shard_map/gla_backward/pallas_call | solution.py:461
  47.4 0.8 %finish.1 = (bf16[256,128]{1,0:T(8,128)(2,1)}, bf16[256,128]{1,0:T(8,128)(2,1)}, f32[256,128]{1,0:T(8,128)}, f32[64,256]{1,0:T(8,128)}, f32[1,64]{1,0:T(1,128)}) custom-call(bf16[256,128]{1,0:T(8,128)(2,1)S(1)} %get-tuple-element.15.refs_0_, bf16[256,128]{1,0:T(8,128)(2,1)S(1)} %get-tuple-element.16.refs_1_, f32[256,128]{1,0:T(8,128)S(1)} %get-tuple-element.17.refs_2_, ...), custom_call_target="tpu_custom_call" | custom-call | tf_op jit(solution)/shard_map/finish/pallas_call | solution.py:487

commit v8 on v7

--- a/solution.py
+++ b/solution.py
@@ -13,7 +13,7 @@
 NZ, NX, NT = 8, 4, 8
 SLAB = DV // NX
 ROWS = 64
-X1, Z2, XI, X3, GX, XX, XY, XC, RZ, TP = 0, 2, 3, 4, 6, 7, 8, 9, 10, 12
+X1, Z2, XI, X3, GX, XX, RZ, TP = 0, 2, 3, 4, 6, 7, 8, 10
 MESH = pl.DeviceIdType.MESH
 F32, BF16 = jnp.float32, jnp.bfloat16
 
@@ -256,11 +256,11 @@
 
     def xy_copy(j, k, slot, to):
         ref = xg.at[slot, k]
-        return remote(ref, ref, sent.at[XY], xy_rs.at[j - 1, k], tp_dev(to))
+        return remote(ref, ref, sent.at[XX], xy_rs.at[j - 1, k], tp_dev(to))
 
     def xc_copy(k, slot):
         ref = xg.at[slot, k]
-        return remote(ref, ref, sent.at[XC], xc_rs.at[0], tp_dev(sibling))
+        return remote(ref, ref, sent.at[XX], xc_rs.at[0], tp_dev(sibling))
 
     for k in (1, 3, 2):
         xx_copy(k, lax.rem(x + NX - k, NX)).wait_recv()
@@ -268,34 +268,6 @@
             xy_copy(j, 3 - k, tp, lax.rem(tp + 2 * j, NT)).start()
         xc_copy(3 - k, tp).start()
 
-    arrived(xir.at[pl.ds(0, 3)], xi_rs.at[0])
-    adj_row = xir[...].reshape(DV, DK)
-    row_vg = local_vg + dot_nt(k_end.astype(BF16), adj_row.astype(BF16))
-    for h in range(2):
-        for p in range(2):
-            gx[x, 2 * h + p] = row_vg[p * 128 : (p + 1) * 128, h * DK : (h + 1) * DK]
-    gx_own(1)
-    gx_forward(0)
-
-    def adj_step(n, acc):
-        t = NZ - 1 - n
-        z_copy(0, t, t).wait_recv()
-        return z2r[0, t, :SLAB, :] + z2r[0, t, SLAB : SLAB + 1, :] * acc
-
-    x3s[0, 0] = lax.fori_loop(0, NZ - 1 - z, adj_step, jnp.zeros((SLAB, DK), F32))
-
-    def x3_copy(i, src, slot, to):
-        return remote(x3s.at[i, src], x3r.at[i, slot], sent.at[X3 + i], x3_rs.at[i], x_dev(to))
-
-    def x3_wait(i):
-        arrived(x3r.at[i, pl.ds(0, 3)], x3_rs.at[i])
-
-    for k in (2, 1, 3):
-        x3_copy(0, 0, x, lax.rem(x + k, NX)).start()
-    x3r[0, x] = x3s[0, 0]
-
-    gx_forward(1)
-    gx_own(2)
     x_leg_wait(1)
     acc = slab(1, 0)
     for t in range(1, NX):
@@ -307,6 +279,34 @@
         def _():
             z_copy(1, z + k, z).start()
 
+    arrived(xir.at[pl.ds(0, 3)], xi_rs.at[0])
+    adj_row = xir[...].reshape(DV, DK)
+    row_vg = local_vg + dot_nt(k_end.astype(BF16), adj_row.astype(BF16))
+    for h in range(2):
+        for p in range(2):
+            gx[x, 2 * h + p] = row_vg[p * 128 : (p + 1) * 128, h * DK : (h + 1) * DK]
+    gx_own(1)
+    gx_forward(0)
+
+    def adj_step(n, acc):
+        t = NZ - 1 - n
+        z_copy(0, t, t).wait_recv()
+        return z2r[0, t, :SLAB, :] + z2r[0, t, SLAB : SLAB + 1, :] * acc
+
+    x3s[0, 0] = lax.fori_loop(0, NZ - 1 - z, adj_step, jnp.zeros((SLAB, DK), F32))
+
+    def x3_copy(i, src, slot, to):
+        return remote(x3s.at[i, src], x3r.at[i, slot], sent.at[X3 + i], x3_rs.at[i], x_dev(to))
+
+    def x3_wait(i):
+        arrived(x3r.at[i, pl.ds(0, 3)], x3_rs.at[i])
+
+    for k in (2, 1, 3):
+        x3_copy(0, 0, x, lax.rem(x + k, NX)).start()
+    x3r[0, x] = x3s[0, 0]
+
+    gx_forward(1)
+    gx_own(2)
     for k in (1, 3, 2):
         for j in (1, 3, 2):
             slot = lax.rem(tp + NT - 2 * j, NT)
@@ -324,17 +324,20 @@
     def rz_copy(h, src, slot, to):
         return remote(dwp.at[h, src], rzr.at[h, slot], sent.at[RZ + h], rz_rs.at[h], z_dev(to))
 
-    def product(h, t):
-        k_t = gx[t, 4:6].reshape(T, DK).astype(BF16)
-        a_t = as_v[t, h * DK : (h + 1) * DK].astype(BF16)
-        vg = (gx[t, 2 * h : 2 * h + 2].reshape(T, DK) + dot_nt(k_t, a_t)).astype(BF16)
+    def entering(h, t):
+        return dot_nt(gx[t, 4:6].reshape(T, DK).astype(BF16), as_v[t, h * DK : (h + 1) * DK].astype(BF16))
+
+    def product(h, t, late):
+        vg = (gx[t, 2 * h : 2 * h + 2].reshape(T, DK) + late).astype(BF16)
         return dot(xb_v[:, :, columns(t)].reshape(NZ * ROWS, T), vg)
 
     def half_product(h):
+        mine, late_far = entering(h, x), entering(h, far)
+        late_left, late_right = entering(h, left), entering(h, right)
         gx_wait(gx_rest, h + 1)
-        near = product(h, x) + product(h, left) + product(h, right)
+        near = product(h, x, mine) + product(h, left, late_left) + product(h, right, late_right)
         gx_wait(gx_far, h + 1)
-        dwp[h] = (near + product(h, far)).reshape(NZ, ROWS, DK)
+        dwp[h] = (near + product(h, far, late_far)).reshape(NZ, ROWS, DK)
         for k in (4, 3, 5, 2, 6, 1, 7):
             t = lax.rem(z + k, NZ)
             rz_copy(h, t, z, t).start()
@@ -403,9 +406,7 @@
     left_here(x3r.at[0, pl.ds(0, 3)], sent.at[X3])
     left_here(x3r.at[1, pl.ds(0, 3)], sent.at[X3 + 1])
     left_here(gx.at[pl.ds(0, 3)], sent.at[GX])
-    left_here(xts.at[pl.ds(0, 3)], sent.at[XX])
-    left_here(xg.at[pl.ds(0, 3)], sent.at[XY])
-    left_here(xg.at[pl.ds(0, 4)], sent.at[XC])
+    left_here(xg, sent.at[XX])
     for store in stores[:3]:
         store.wait()
 
@@ -425,7 +426,7 @@
     def tp_copy(slot, to):
         return remote(tps, tpr.at[slot], sent.at[TP], tp_rs.at[0], tp_dev(to))
 
-    for k in range(1, NT):
+    for k in (4, 5, 3, 2, 6, 7, 1):
         tp_copy(tp, lax.rem(tp + k, NT)).start()
     left_here(dwp.at[0, pl.ds(0, 7)], sent.at[RZ])
     left_here(dwp.at[1, pl.ds(0, 7)], sent.at[RZ + 1])
@@ -478,7 +479,7 @@
             vmem((NX, 6, T // 2, DK), F32), vmem((NX, ROWS, T), F32), vmem((NT, NX - 1, ROWS, T), F32),
             vmem((2, NZ, ROWS, DK), F32), vmem((2, NZ, ROWS, DK), F32),
             vmem((8, 128), F32), vmem((NT, 8, 128), F32),
-            dma((6,)), dma((5,)), dma((13,)), dma((2,)), dma((NZ,)), dma((1,)), dma((2,)), dma((2, 4)), dma((3,)),
+            dma((6,)), dma((5,)), dma((11,)), dma((2,)), dma((NZ,)), dma((1,)), dma((2,)), dma((2, 4)), dma((3,)),
             dma((3,)), dma((3,)), dma((3, 3)), dma((1,)), dma((2,)), dma((1,)),
         ],
         compiler_params=pltpu.CompilerParams(collective_id=0, has_side_effects=True, vmem_limit_bytes=40 << 20),

time: 48.3 us -> 48 us (level)
  no operation moved by 1% of the time
where the time goes in v8:
time: 48 us; the launch traced here: 47.9 us
  Pallas kernels  47.3 us (99%)
  between operations  0.64 us (1%)
    pallas_call x1, Pallas kernels, on_device(): pl.pallas_call(kernel, out_shape=tuple((vmem(*s) for s in shapes)), in_sp...  46.5 us

profile of v8, /device:TPU:1, one launch (start us, length us, event | category | flops | bytes accessed | tf_op | source)
XLA Modules:
  0.0 47.9 jit_solution(7071575819785075824)
XLA Ops:
  0.6 46.5 %gla_backward.1 = (bf16[256,128]{1,0:T(8,128)(2,1)S(1)}, bf16[256,128]{1,0:T(8,128)(2,1)S(1)}, f32[256,128]{1,0:T(8,128)S(1)}, f32[64,256]{1,0:T(8,128)S(1)}, f32[1,64]{1,0:T(1,128)S(1)}) custom-call(bf16[256,2048]{1,0:T(8,128)(2,1)} %x_hbm.1, bf16[256,128]{1,0:T(8,128)(2,1)} %q_hbm.1, bf16[256,128]{1,0:T(8,128)(2,1)} %k_hbm.1, bf16[2048,256]{1,0:T(8,128)(2,1)} %w_hbm.1, ...), custom_call_target="tpu_custom_call" | custom-call | tf_op jit(solution)/shard_map/gla_backward/pallas_call | solution.py:462
  47.2 0.8 %finish.1 = (bf16[256,128]{1,0:T(8,128)(2,1)}, bf16[256,128]{1,0:T(8,128)(2,1)}, f32[256,128]{1,0:T(8,128)}, f32[64,256]{1,0:T(8,128)}, f32[1,64]{1,0:T(1,128)}) custom-call(bf16[256,128]{1,0:T(8,128)(2,1)S(1)} %get-tuple-element.15.refs_0_, bf16[256,128]{1,0:T(8,128)(2,1)S(1)} %get-tuple-element.16.refs_1_, f32[256,128]{1,0:T(8,128)S(1)} %get-tuple-element.17.refs_2_, ...), custom_call_target="tpu_custom_call" | custom-call | tf_op jit(solution)/shard_map/finish/pallas_call | solution.py:488
